TPU v7x, 512 devices: a whole 4x4x16 slice. The times are simulated.
512 devices in a mesh: ep: 128 (over z, x, core), tp: 4 (over y).
Axes of the slice: x: 4, y: 4, z: 16, core: 2. Of those that a mesh axis runs over, the one named last changes fastest.
Arguments:
- residual: bfloat16 [2048, 1024], P('ep', 'tp'), may hold values from -32 to 32
- cache_keys: bfloat16 [2048, 1024, 256], P(('ep', 'tp')), may hold values from -128 to 128
- cache_values: bfloat16 [2048, 1024, 256], P(('ep', 'tp')), may hold values from -6 to 6
- lengths: int32 [2048], P('ep'), may hold values from 128 to 1024
- query_weight: bfloat16 [1024, 1024], P('tp', 'ep'), may hold values from -0.1875 to 0.1875
- key_weight: bfloat16 [1024, 256], P('tp', 'ep'), may hold values from -0.1875 to 0.1875
- value_weight: bfloat16 [1024, 256], P('tp', 'ep'), may hold values from -0.1875 to 0.1875
- out_weight: bfloat16 [1024, 1024], P('tp', 'ep'), may hold values from -0.1875 to 0.1875
- head_gain: float32 [128], replicated, may hold values from 0.1 to 1.9
- mix_lambda: float32 [8], replicated, may hold values from 0.3 to 0.8
- attn_gain: bfloat16 [1024], P('tp'), may hold values from 0.099609375 to 1.8984375
- moe_gain: bfloat16 [1024], P('tp'), may hold values from 0.099609375 to 1.8984375
- route_ids: int32 [2048, 6], P('ep'), may hold values from 0 to 127, as said below
- route_logits: float32 [2048, 6], P('ep'), may hold values from -8 to 8
- gate_weight: bfloat16 [128, 1024, 512], P('ep', None, 'tp'), may hold values from -0.1875 to 0.1875
- up_weight: bfloat16 [128, 1024, 512], P('ep', None, 'tp'), may hold values from -0.1875 to 0.1875
- down_weight: bfloat16 [128, 512, 1024], P('ep', 'tp'), may hold values from -1.5 to 1.5
Outputs:
- output: bfloat16 [2048, 1024], P('ep', 'tp')
- new_keys: bfloat16 [2048, 256], P('ep')
- new_values: bfloat16 [2048, 256], P('ep')
Inputs may be any that keep to these rules, and one draw needn't show every extreme that they name: `route_ids`: the 6 experts of a row are distinct and lie in one group of 8 consecutive experts. Among the 16 rows of one index of ep, no expert is named by more than 2 rows, and some expert is named by exactly 2 of them.
All inputs are finite; a program needn't handle non-finite values.
Results may differ from a plain program's by a relative error of at most 0.013.
The roundings to bfloat16 on the way count: a program that leaves them out, or rounds other values in their place, can miss the bound.
Values may be sent and summed in bfloat16 or wider, within the bound.
A program may use at most 64 MiB of HBM per device.

v0:
```python
import jax
import jax.numpy as jnp
from jax import lax
from jax.sharding import Mesh
from jax.sharding import PartitionSpec as P

WIDTH = 1024
HEADS = 8
KV_HEADS = 2
HEAD_DIM = 64
VALUE_DIM = 128
GROUP_SIZE = 8
CHOSEN = 6
EP = ("ep_0", "ep_1", "ep_2")
EP_TP = ("ep_0", "ep_1", "ep_2", "tp")


norm_eps = 1e-06
head_eps = 1e-05
masked_score = -1e30
rotary_base = 500000.0


def joined_along(tiles, dim):
    tiles = jnp.moveaxis(tiles, 0, dim)
    dims = tiles.shape
    return tiles.reshape(*dims[:dim], dims[dim] * dims[dim + 1], *dims[dim + 2 :])


def all_blocks(value, axes, turns):
    tiles = value
    for k in turns:
        tiles = lax.all_gather(tiles, axes[k])
    done = turns[::-1]
    back = [done.index(k) for k in range(len(axes))]
    tiles = tiles.transpose(*back, *range(len(axes), tiles.ndim))
    return tiles.reshape(-1, *value.shape)


def whole_of(value, axes, turns, dim):
    return joined_along(all_blocks(value, axes, turns), dim)


def cut_along(value, dim, devices):
    dims = value.shape
    tiles = value.reshape(*dims[:dim], devices, dims[dim] // devices, *dims[dim + 1 :])
    return jnp.moveaxis(tiles, dim, 0)


def sum_at_owner(value, axis, dim):
    tiles = cut_along(value, dim, lax.axis_size(axis))
    arrived = lax.all_to_all(tiles, axis, split_axis=0, concat_axis=0, tiled=True)
    return arrived.sum(axis=0)


def rotate(blocks, positions):
    half_dim = blocks.shape[-1] // 2
    inverse = rotary_base ** (-jnp.arange(half_dim, dtype=jnp.float32) / half_dim)
    angles = positions[:, None] * inverse[None, :]
    cosine = jnp.cos(angles)[:, None, :]
    sine = jnp.sin(angles)[:, None, :]
    first_half = blocks[..., :half_dim]
    second_half = blocks[..., half_dim:]
    return jnp.concatenate(
        [first_half * cosine - second_half * sine, second_half * cosine + first_half * sine],
        axis=-1,
    )


def on_device(
    residual,
    cache_keys,
    cache_values,
    lengths,
    query_weight,
    key_weight,
    value_weight,
    out_weight,
    head_gain,
    mix_lambda,
    attn_gain,
    moe_gain,
    route_ids,
    route_logits,
    gate_weight,
    up_weight,
    down_weight,
):
    ep_count = lax.axis_size(EP)
    tp_index = lax.axis_index("tp")
    seq_count = residual.shape[0]
    groups_per = HEADS // KV_HEADS
    stream = residual.astype(jnp.float32)
    squares = lax.psum(jnp.sum(stream * stream, axis=1), "tp")
    normed = (
        stream * lax.rsqrt(squares / WIDTH + norm_eps)[:, None] * attn_gain.astype(jnp.float32)
    ).astype(jnp.bfloat16)
    joined = jnp.concatenate([query_weight, key_weight, value_weight], axis=1)
    partial_cols = jnp.dot(
        normed, whole_of(joined, EP, (1, 0, 2), 1), preferred_element_type=jnp.float32
    )
    projected = lax.psum(partial_cols, "tp")
    query_cols = query_weight.shape[1]
    key_cols = key_weight.shape[1]
    per_source = projected.reshape(seq_count, ep_count, -1)
    query_raw = per_source[:, :, :query_cols].reshape(seq_count, 2 * HEADS, HEAD_DIM)
    key_raw = per_source[:, :, query_cols : query_cols + key_cols].reshape(
        seq_count, 2 * KV_HEADS, HEAD_DIM
    )
    value_raw = per_source[:, :, query_cols + key_cols :].reshape(seq_count, KV_HEADS * VALUE_DIM)
    positions = lengths.astype(jnp.float32)
    queries = (
        rotate(query_raw, positions)
        .astype(jnp.bfloat16)
        .reshape(seq_count, KV_HEADS, groups_per, 2, HEAD_DIM)
    )
    new_keys = rotate(key_raw, positions).astype(jnp.bfloat16)
    new_values = value_raw.astype(jnp.bfloat16)
    key_heads = new_keys.reshape(seq_count, KV_HEADS, 2, HEAD_DIM)
    value_heads = new_values.reshape(seq_count, KV_HEADS, VALUE_DIM)
    own_count = cache_keys.shape[0]
    cache_length = cache_keys.shape[1]
    own_start = tp_index * own_count
    own_queries = lax.dynamic_slice_in_dim(queries, own_start, own_count, 0)
    own_keys = lax.dynamic_slice_in_dim(key_heads, own_start, own_count, 0)
    own_values = lax.dynamic_slice_in_dim(value_heads, own_start, own_count, 0)
    own_lengths = lax.dynamic_slice_in_dim(lengths, own_start, own_count, 0)
    cached_keys = cache_keys.reshape(own_count, cache_length, KV_HEADS, 2, HEAD_DIM)
    cached_values = cache_values.reshape(own_count, cache_length, KV_HEADS, VALUE_DIM)
    cache_scores = (
        jnp.einsum(
            "bkgmd,blkmd->bkgml", own_queries, cached_keys, preferred_element_type=jnp.float32
        )
        * 0.125
    )
    valid = jnp.arange(cache_length, dtype=jnp.int32)[None, :] < own_lengths[:, None]
    cache_scores = jnp.where(valid[:, None, None, None, :], cache_scores, masked_score)
    own_scores = (
        jnp.einsum("bkgmd,bkmd->bkgm", own_queries, own_keys, preferred_element_type=jnp.float32)
        * 0.125
    )
    maxima = jnp.maximum(jnp.max(cache_scores, axis=-1), own_scores)
    cache_weights = jnp.exp(cache_scores - maxima[..., None]).astype(jnp.bfloat16)
    own_weights = jnp.exp(own_scores - maxima).astype(jnp.bfloat16).astype(jnp.float32)
    denominator = jnp.sum(cache_weights.astype(jnp.float32), axis=-1) + own_weights
    weighted = jnp.einsum(
        "bkgml,blkv->bkgmv", cache_weights, cached_values, preferred_element_type=jnp.float32
    )
    weighted = (
        weighted + own_weights[..., None] * own_values.astype(jnp.float32)[:, :, None, None, :]
    )
    averaged = weighted / denominator[..., None]
    lambdas = mix_lambda.reshape(KV_HEADS, groups_per)[None, :, :, None]
    contrast = averaged[:, :, :, 0] - lambdas * averaged[:, :, :, 1]
    contrast = (
        contrast
        * lax.rsqrt(jnp.mean(contrast * contrast, axis=-1, keepdims=True) + head_eps)
        * head_gain
    )
    heads_out = contrast.astype(jnp.bfloat16).reshape(own_count, HEADS * VALUE_DIM)
    own_heads = lax.all_to_all(heads_out, "tp", split_axis=1, concat_axis=0, tiled=True)
    partial_out = jnp.dot(
        own_heads, whole_of(out_weight, EP, (1, 0, 2), 1), preferred_element_type=jnp.float32
    )
    attended = sum_at_owner(partial_out, "tp", 1)
    middle = (stream + attended).astype(jnp.bfloat16)
    middle_wide = middle.astype(jnp.float32)
    squares_moe = lax.psum(jnp.sum(middle_wide * middle_wide, axis=1), "tp")
    mixed_in = (
        middle_wide
        * lax.rsqrt(squares_moe / WIDTH + norm_eps)[:, None]
        * moe_gain.astype(jnp.float32)
    ).astype(jnp.bfloat16)
    group_count = ep_count // GROUP_SIZE
    group_most = min(seq_count, max(2, -(-seq_count // group_count)))
    capacity = (CHOSEN * group_most + GROUP_SIZE - 1) // GROUP_SIZE
    expert_ids = route_ids.reshape(-1)
    pair_count = expert_ids.shape[0]
    matches = expert_ids[:, None] == expert_ids[None, :]
    earlier = jnp.arange(pair_count)[:, None] > jnp.arange(pair_count)[None, :]
    slot_rank = jnp.sum(jnp.logical_and(matches, earlier), axis=1)
    slot_index = expert_ids * capacity + slot_rank
    onehot = (
        slot_index[:, None] == jnp.arange(ep_count * capacity, dtype=jnp.int32)[None, :]
    ).reshape(seq_count, CHOSEN, ep_count * capacity)
    dispatch = jnp.sum(onehot.astype(jnp.bfloat16), axis=1)
    outgoing = jnp.einsum(
        "te,td->ed", dispatch, mixed_in, preferred_element_type=jnp.float32
    ).astype(jnp.bfloat16)
    outgoing = outgoing.reshape(ep_count, capacity, -1)
    received = lax.all_to_all(outgoing, EP, split_axis=0, concat_axis=0, tiled=True)
    received = lax.all_gather(received, "tp", axis=2, tiled=True)
    flattened = received.reshape(-1, received.shape[2])
    gate_act = jnp.dot(flattened, gate_weight[0], preferred_element_type=jnp.float32)
    up_act = jnp.dot(flattened, up_weight[0], preferred_element_type=jnp.float32)
    hidden = (jax.nn.silu(gate_act) * up_act).astype(jnp.bfloat16)
    produced = jnp.dot(hidden, down_weight[0], preferred_element_type=jnp.float32).reshape(
        received.shape
    )
    summed = sum_at_owner(produced, "tp", 2)
    returned = lax.all_to_all(
        summed.astype(jnp.bfloat16), EP, split_axis=0, concat_axis=0, tiled=True
    )
    gates = jax.nn.softmax(route_logits, axis=-1)
    combine = jnp.einsum(
        "tke,tk->te", onehot.astype(jnp.float32), gates, precision=lax.Precision.HIGHEST
    )
    expert_mix = jnp.dot(
        combine,
        returned.reshape(ep_count * capacity, -1).astype(jnp.float32),
        precision=lax.Precision.HIGHEST,
    )
    output = (middle_wide + expert_mix).astype(jnp.bfloat16)
    return (output, new_keys.reshape(seq_count, -1), new_values)


def solution(mesh):
    torus = Mesh(mesh.devices.reshape(16, 4, 2, mesh.shape["tp"]), ("ep_0", "ep_1", "ep_2", "tp"))
    return jax.shard_map(
        on_device,
        mesh=torus,
        in_specs=(
            P(EP, "tp"),
            P(EP_TP, None, None),
            P(EP_TP, None, None),
            P(EP),
            P("tp", EP),
            P("tp", EP),
            P("tp", EP),
            P("tp", EP),
            P(),
            P(),
            P("tp"),
            P("tp"),
            P(EP, None),
            P(EP, None),
            P(EP, None, "tp"),
            P(EP, None, "tp"),
            P(EP, "tp", None),
        ),
        out_specs=(P(EP, "tp"), P(EP, None), P(EP, None)),
        check_vma=False,
    )
```

profile of v0, /device:TPU:1, one launch (start us, length us, event | category | flops | bytes accessed | tf_op | source)
XLA Modules:
  0.0 260.4 jit_solution(16974086310599921868)
XLA Ops:
  7.2 0.8 pad_maximum_fusion.1
  8.0 10.2 %all-gather = bf16[1024,12]{0,1:T(8,128)(2,1)S(1)} all-gather(bf16[256,12]{0,1:T(8,128)(2,1)S(1)} %pad_maximum_fusion.1), channel_id=2, replica_groups=mesh['ep_0'=16,'ep_1'=4,'ep_2'=2,'tp'=4] {'ep_1'}, dimensions={0}, use_global_device_ids=true | all-gather | bytes 30720 | tf_op jit(solution)/shard_map/all_gather | solution.py:33
  18.2 31.0 %all-gather.1 = bf16[64,256,12]{1,2,0:T(8,128)(2,1)S(1)} all-gather(bf16[4,256,12]{1,2,0:T(8,128)(2,1)S(1)} %copy.250), channel_id=3, replica_groups=mesh['ep_0'=16,'ep_1'=4,'ep_2'=2,'tp'=4] {'ep_0'}, dimensions={0}, use_global_device_ids=true | all-gather | bytes 417792 | tf_op jit(solution)/shard_map/all_gather | solution.py:33
  49.4 12.8 %all-gather.2 = bf16[32,4,256,12]{2,1,0,3:T(4,128)(2,1)S(1)} all-gather(bf16[16,4,256,12]{2,1,0,3:T(4,128)(2,1)S(1)} %copy.289), channel_id=4, replica_groups=mesh['ep_0'=16,'ep_1'=4,'ep_2'=2,'tp'=4] {'ep_2'}, dimensions={0}, use_global_device_ids=true | all-gather | bytes 1179648 | tf_op jit(solution)/shard_map/all_gather | solution.py:33
  62.3 0.7 copy.253
  63.0 0.3 reshape.194
  63.4 0.5 copy.254
  64.2 8.7 %psum.21 = f32[16]{0:T(128)S(1)} all-reduce(f32[16]{0:T(128)S(1)} %fusion.20), channel_id=1, replica_groups=mesh['ep_0'=16,'ep_1'=4,'ep_2'=2,'tp'=4] {'tp'}, use_global_device_ids=true, to_apply=%region_1.0 | all-reduce | flops 16 | bytes 128 | tf_op jit(solution)/shard_map/psum | solution.py:94
  72.9 0.3 fusion.32
  73.2 1.1 reshape.196
  74.4 1.0 copy.255
  75.6 3.0 %copy.261 = bf16[4,1024,256]{1,2,0:T(8,128)(2,1)S(1)} copy(bf16[4,1024,256]{2,1,0:T(8,128)(2,1)} %param.18) | data formatting | bytes 4194304 | tf_op args[1]
  78.6 4.0 %reshape.200 = bf16[4,1024,2,128]{3,2,1,0:T(2,128)(2,1)} reshape(bf16[4,1024,256]{2,1,0:T(8,128)(2,1)} %param.19) | data formatting | bytes 4194304 | tf_op jit(solution)/shard_map/reshape | solution.py:129
  82.7 0.6 mul.250
  83.4 0.6 mul.260
  84.0 9.7 %all-gather.3 = bf16[1024,8]{0,1:T(8,128)(2,1)S(1)} all-gather(bf16[256,8]{0,1:T(8,128)(2,1)S(1)} %copy-done.7), channel_id=5, replica_groups=mesh['ep_0'=16,'ep_1'=4,'ep_2'=2,'tp'=4] {'ep_1'}, dimensions={0}, use_global_device_ids=true | all-gather | bytes 20480 | tf_op jit(solution)/shard_map/all_gather | solution.py:33
  94.4 20.8 %all-gather.4 = bf16[64,256,8]{1,2,0:T(8,128)(2,1)S(1)} all-gather(bf16[4,256,8]{1,2,0:T(8,128)(2,1)S(1)} %bitcast.127), channel_id=6, replica_groups=mesh['ep_0'=16,'ep_1'=4,'ep_2'=2,'tp'=4] {'ep_0'}, dimensions={0}, use_global_device_ids=true | all-gather | bytes 278528 | tf_op jit(solution)/shard_map/all_gather | solution.py:33
  115.1 9.9 %all-reduce.2.cloned.1.call-done = f32[16,128,12]{1,0,2:T(8,128)} async-done(((f32[16,128,12]{1,0,2:T(8,128)}), f32[16,128,12]{1,0,2:T(8,128)}) %all-reduce.2.cloned.1.call-update) | async-done | bytes 98320 | tf_op jit(solution)/shard_map/psum | solution.py:102
  125.0 0.7 slice.39
  125.9 0.7 copy.263
  126.5 0.7 copy.264
  127.2 0.8 slice.36
  128.7 0.8 fusion.44
  129.7 0.5 fusion.50
  130.5 0.7 slice.57
  131.5 2.1 fusion.8
  134.0 0.6 copy.270
  134.6 3.4 %all-to-all-start = ((bf16[4,4,256]{2,0,1:T(4,128)(2,1)}), bf16[4,4,256]{2,0,1:T(4,128)(2,1)S(1)}, u32[]{:S(2)}, u32[]{:S(2)}) async-start(bf16[4,4,256]{2,0,1:T(4,128)(2,1)} %copy.270), calls=%async_computation | async-start | bytes 16384 | tf_op jit(solution)/shard_map/all_to_all | solution.py:161
  138.0 4.5 %all-gather.5 = bf16[32,4,256,8]{2,3,1,0:T(8,128)(2,1)S(1)} all-gather(bf16[16,4,256,8]{2,3,1,0:T(8,128)(2,1)S(1)} %bitcast.116), channel_id=7, replica_groups=mesh['ep_0'=16,'ep_1'=4,'ep_2'=2,'tp'=4] {'ep_2'}, dimensions={0}, use_global_device_ids=true | all-gather | bytes 786432 | tf_op jit(solution)/shard_map/all_gather | solution.py:33
  142.6 0.9 convolution_bitcast_fusion.1
  143.5 4.6 %all-to-all-start.1 = ((f32[4,16,256]{2,1,0:T(8,128)}), f32[4,16,256]{2,1,0:T(8,128)S(1)}, u32[]{:S(2)}, u32[]{:S(2)}) async-start(f32[4,16,256]{2,1,0:T(8,128)} %convolution_bitcast_fusion.1), calls=%async_computation.1 | async-start | bytes 131072 | tf_op jit(solution)/shard_map/all_to_all | solution.py:52
  148.2 4.4 %all-to-all-done.1 = f32[4,16,256]{2,1,0:T(8,128)S(1)} async-done(((f32[4,16,256]{2,1,0:T(8,128)}), f32[4,16,256]{2,1,0:T(8,128)S(1)}, u32[]{:S(2)}, u32[]{:S(2)}) %all-to-all-start.1) | async-done | bytes 65568 | tf_op jit(solution)/shard_map/all_to_all | solution.py:52
  152.7 6.9 %psum.23 = f32[16]{0:T(128)S(1)} all-reduce(f32[16]{0:T(128)S(1)} %get-tuple-element.30), channel_id=1, replica_groups=mesh['ep_0'=16,'ep_1'=4,'ep_2'=2,'tp'=4] {'tp'}, use_global_device_ids=true, to_apply=%region_12.13 | all-reduce | flops 16 | bytes 128 | tf_op jit(solution)/shard_map/psum | solution.py:168
  159.9 0.7 reshape.203
  160.6 21.3 %all-to-all-start.2 = ((bf16[128,2,256]{2,1,0:T(2,128)(2,1)}), bf16[128,2,256]{2,1,0:T(2,128)(2,1)S(1)}, u32[]{:S(2)}, u32[]{:S(2)}) async-start(bf16[128,2,256]{2,1,0:T(2,128)(2,1)} %reshape.203), calls=%async_computation.2 | async-start | bytes 262144 | tf_op jit(solution)/shard_map/all_to_all | solution.py:191
  182.1 15.8 %all-to-all-done.2 = bf16[128,2,256]{2,1,0:T(2,128)(2,1)S(1)} async-done(((bf16[128,2,256]{2,1,0:T(2,128)(2,1)}), bf16[128,2,256]{2,1,0:T(2,128)(2,1)S(1)}, u32[]{:S(2)}, u32[]{:S(2)}) %all-to-all-start.2) | async-done | bytes 131104 | tf_op jit(solution)/shard_map/all_to_all | solution.py:191
  197.9 9.4 %all_gather.51 = bf16[128,2,1024]{2,1,0:T(2,128)(2,1)S(1)} all-gather(bf16[128,2,256]{2,1,0:T(2,128)(2,1)S(1)} %all-to-all-done.2), channel_id=1, replica_groups=mesh['ep_0'=16,'ep_1'=4,'ep_2'=2,'tp'=4] {'tp'}, dimensions={2}, use_global_device_ids=true | all-gather | bytes 655360 | tf_op jit(solution)/shard_map/all_gather | solution.py:192
  207.8 0.3 fusion.4
  208.1 0.3 convolution_bitcast_fusion
  208.4 1.1 copy.276
  209.5 3.5 %all-to-all-start.3 = ((f32[4,128,2,256]{3,1,2,0:T(8,128)}), f32[4,128,2,256]{3,1,2,0:T(8,128)S(1)}, u32[]{:S(2)}, u32[]{:S(2)}) async-start(f32[4,128,2,256]{3,1,2,0:T(8,128)} %copy.276), calls=%async_computation.3 | async-start | bytes 2097152 | tf_op jit(solution)/shard_map/all_to_all | solution.py:52
  213.2 12.9 %all-to-all-done.3 = f32[4,128,2,256]{3,1,2,0:T(8,128)S(1)} async-done(((f32[4,128,2,256]{3,1,2,0:T(8,128)}), f32[4,128,2,256]{3,1,2,0:T(8,128)S(1)}, u32[]{:S(2)}, u32[]{:S(2)}) %all-to-all-start.3) | async-done | bytes 1048608 | tf_op jit(solution)/shard_map/all_to_all | solution.py:52
  226.1 0.8 copy.278
  226.9 9.8 %all-to-all-start.4 = ((bf16[128,2,256]{2,1,0:T(2,128)(2,1)}), bf16[128,2,256]{2,1,0:T(2,128)(2,1)S(1)}, u32[]{:S(2)}, u32[]{:S(2)}) async-start(bf16[128,2,256]{2,1,0:T(2,128)(2,1)} %copy.278), calls=%async_computation.4 | async-start | bytes 262144 | tf_op jit(solution)/shard_map/all_to_all | solution.py:201
  237.1 0.7 copy.299
  237.7 0.7 copy.281
  238.4 14.3 %all-to-all-done.4 = bf16[128,2,256]{2,1,0:T(2,128)(2,1)S(1)} async-done(((bf16[128,2,256]{2,1,0:T(2,128)(2,1)}), bf16[128,2,256]{2,1,0:T(2,128)(2,1)S(1)}, u32[]{:S(2)}, u32[]{:S(2)}) %all-to-all-start.4) | async-done | bytes 131104 | tf_op jit(solution)/shard_map/all_to_all | solution.py:201
  252.8 0.8 fusion.11
  (99 shorter events, 5.4 us)
Async XLA Ops:
  7.2 200.3 %copy-start = (bf16[1,1024,128]{2,1,0:T(8,128)(2,1)S(1)}, bf16[1,1024,128]{2,1,0:T(8,128)(2,1)}, u32[]{:S(2)}) copy-start(bf16[1,1024,128]{2,1,0:T(8,128)(2,1)} %param.31) | copy-start | bytes 786436
  7.2 117.8 %all-reduce.2.cloned.1.call-start = ((), (), s32[]{:S(2)}) async-start(), calls=%async_computation.5 | async-start | bytes 196608 | tf_op jit(solution)/shard_map/psum | solution.py:102
  63.3 0.7 copy-start.2
  63.3 9.5 %copy-start.12 = (bf16[256]{0:T(256)(128)(2,1)S(1)}, bf16[256]{0:T(256)(128)(2,1)}, u32[]{:S(2)}) copy-start(bf16[256]{0:T(256)(128)(2,1)} %param.27) | copy-start | bytes 1540
  64.0 11.3 %copy-start.13 = (s32[16]{0:T(128)S(1)}, s32[16]{0:T(128)}, u32[]{:S(2)}) copy-start(s32[16]{0:T(128)} %param.20) | copy-start | bytes 196
  78.5 4.0 %copy-start.14 = (f32[8]{0:T(128)S(1)}, f32[8]{0:T(128)}, u32[]{:S(2)}) copy-start(f32[8]{0:T(128)} %param.26) | copy-start | bytes 100
  78.6 4.8 %copy-start.10 = (f32[128]{0:T(128)S(1)}, f32[128]{0:T(128)}, u32[]{:S(2)}) copy-start(f32[128]{0:T(128)} %param.25) | copy-start | bytes 1540
  78.6 5.4 %copy-start.7 = (bf16[256,8]{0,1:T(8,128)(2,1)S(1)}, bf16[256,8]{0,1:T(8,128)(2,1)}, u32[]{:S(2)}) copy-start(bf16[256,8]{0,1:T(8,128)(2,1)} %param.24) | copy-start | bytes 12292
  78.6 15.1 %copy-start.4 = (s32[16,6]{0,1:T(8,128)S(1)}, s32[16,6]{0,1:T(8,128)}, u32[]{:S(2)}) copy-start(s32[16,6]{0,1:T(8,128)} %param.29) | copy-start | bytes 1156
  82.7 1.3 copy-start.8
  130.2 3.5 %copy-start.9 = (f32[2,4]{1,0:T(2,128)S(1)}, f32[2,4]{1,0:T(2,128)}, u32[]{:S(2)}) copy-start(f32[2,4]{1,0:T(2,128)} %copy-done.8) | copy-start | bytes 100
  130.2 3.8 %copy-start.5 = (f32[4,256]{1,0:T(4,128)S(1)}, f32[4,256]{1,0:T(4,128)}, u32[]{:S(2)}) copy-start(f32[4,256]{1,0:T(4,128)} %mul.250) | copy-start | bytes 12292
  130.2 3.8 %copy-start.6 = (f32[4,256]{1,0:T(4,128)S(1)}, f32[4,256]{1,0:T(4,128)}, u32[]{:S(2)}) copy-start(f32[4,256]{1,0:T(4,128)} %mul.260) | copy-start | bytes 12292
  133.6 14.6 %copy-start.15 = (bf16[256]{0:T(256)(128)(2,1)S(1)}, bf16[256]{0:T(256)(128)(2,1)}, u32[]{:S(2)}) copy-start(bf16[256]{0:T(256)(128)(2,1)} %param.28) | copy-start | bytes 1540
  133.6 48.3 %copy-start.1 = (bf16[1,128,1024]{2,1,0:T(8,128)(2,1)S(1)}, bf16[1,128,1024]{2,1,0:T(8,128)(2,1)}, u32[]{:S(2)}) copy-start(bf16[1,128,1024]{2,1,0:T(8,128)(2,1)} %param.33) | copy-start | bytes 786436
  134.6 8.0 %all-to-all-start = ((bf16[4,4,256]{2,0,1:T(4,128)(2,1)}), bf16[4,4,256]{2,0,1:T(4,128)(2,1)S(1)}, u32[]{:S(2)}, u32[]{:S(2)}) async-start(bf16[4,4,256]{2,0,1:T(4,128)(2,1)} %copy.270), calls=%async_computation | async-start | bytes 16384 | tf_op jit(solution)/shard_map/all_to_all | solution.py:161
  143.5 64.3 %copy-start.11 = (bf16[1,1024,128]{2,1,0:T(8,128)(2,1)S(1)}, bf16[1,1024,128]{2,1,0:T(8,128)(2,1)}, u32[]{:S(2)}) copy-start(bf16[1,1024,128]{2,1,0:T(8,128)(2,1)} %param.32) | copy-start | bytes 786436
  143.5 9.1 %all-to-all-start.1 = ((f32[4,16,256]{2,1,0:T(8,128)}), f32[4,16,256]{2,1,0:T(8,128)S(1)}, u32[]{:S(2)}, u32[]{:S(2)}) async-start(f32[4,16,256]{2,1,0:T(8,128)} %convolution_bitcast_fusion.1), calls=%async_computation.1 | async-start | bytes 131072 | tf_op jit(solution)/shard_map/all_to_all | solution.py:52
  160.6 37.3 %all-to-all-start.2 = ((bf16[128,2,256]{2,1,0:T(2,128)(2,1)}), bf16[128,2,256]{2,1,0:T(2,128)(2,1)S(1)}, u32[]{:S(2)}, u32[]{:S(2)}) async-start(bf16[128,2,256]{2,1,0:T(2,128)(2,1)} %reshape.203), calls=%async_computation.2 | async-start | bytes 262144 | tf_op jit(solution)/shard_map/all_to_all | solution.py:191
  208.4 4.6 %copy-start.3 = (f32[16,6]{0,1:T(8,128)S(1)}, f32[16,6]{0,1:T(8,128)}, u32[]{:S(2)}) copy-start(f32[16,6]{0,1:T(8,128)} %param.30) | copy-start | bytes 1156
  209.5 16.6 %all-to-all-start.3 = ((f32[4,128,2,256]{3,1,2,0:T(8,128)}), f32[4,128,2,256]{3,1,2,0:T(8,128)S(1)}, u32[]{:S(2)}, u32[]{:S(2)}) async-start(f32[4,128,2,256]{3,1,2,0:T(8,128)} %copy.276), calls=%async_computation.3 | async-start | bytes 2097152 | tf_op jit(solution)/shard_map/all_to_all | solution.py:52
  226.9 25.8 %all-to-all-start.4 = ((bf16[128,2,256]{2,1,0:T(2,128)(2,1)}), bf16[128,2,256]{2,1,0:T(2,128)(2,1)S(1)}, u32[]{:S(2)}, u32[]{:S(2)}) async-start(bf16[128,2,256]{2,1,0:T(2,128)(2,1)} %copy.278), calls=%async_computation.4 | async-start | bytes 262144 | tf_op jit(solution)/shard_map/all_to_all | solution.py:201
Sparse Core Ops, SparseCore 0:
  75.5 49.4 all-reduce.1
where the time goes:
time: 261 us; the launch traced here: 260 us
  blocking collectives  114 us (44%)
  waiting for transfers between devices  57.3 us (22%)
  starting transfers between devices  42.7 us (16%)
  local copies, waits for them, and re-layouts  22.6 us (9%)
  between operations  14.5 us (6%)
  matrix products  6.02 us (2%)
  other arithmetic  3.28 us (1%)
    all_gather x6, blocking collectives, all_blocks(): tiles = lax.all_gather(tiles, axes[k])  88.9 us
    all_to_all x1, starting transfers between devices, on_device(): lax.all_to_all(outgoing, EP, split_axis=0, concat_axis=0, tiled=True)  21.3 us
    all_to_all x2, waiting for transfers between devices, sum_at_owner(): lax.all_to_all(tiles, axis, split_axis=0, concat_axis=0, tiled=True)  17.3 us
    all_to_all x1, waiting for transfers between devices, on_device(): lax.all_to_all(outgoing, EP, split_axis=0, concat_axis=0, tiled=True)  15.8 us
    all_to_all x1, waiting for transfers between devices, on_device(): lax.all_to_all(summed.astype(jnp.bfloat16), EP, split_axis=0, concat_axis...  14.3 us
    psum x1, waiting for transfers between devices, on_device(): projected = lax.psum(partial_cols, 'tp')  9.88 us
    all_to_all x1, starting transfers between devices, on_device(): lax.all_to_all(summed.astype(jnp.bfloat16), EP, split_axis=0, concat_axis...  9.85 us
    all_gather x1, blocking collectives, on_device(): received = lax.all_gather(received, 'tp', axis=2, tiled=True)  9.43 us
  transfers between devices with their start and end apart: 6, of which 5 were waited for; matrix products, arithmetic and copies ran while one was open for 4% of the time, Pallas kernels for 0%

commit v1 on v0

v1 whole, which is shorter than its diff:
```python
import jax
import jax.numpy as jnp
from jax import lax
from jax.experimental import pallas as pl
from jax.experimental.pallas import tpu as pltpu
from jax.sharding import Mesh
from jax.sharding import PartitionSpec as P

WIDTH = 1024
HEADS = 8
HEAD_DIM = 64
VALUE_DIM = 128
CHOSEN = 6
GROUP_SIZE = 8
SLOTS = 2
EP = ("ep_0", "ep_1", "ep_2")
EP_TP = ("ep_0", "ep_1", "ep_2", "tp")
NZ, NX, NC, NY = 16, 4, 2, 4
NG = NX * NC
NP = NG * NY
CACHE = 1024
OWN = 4

norm_eps = 1e-06
head_eps = 1e-05
masked_score = -1e30
rotary_base = 500000.0

MESH = pl.DeviceIdType.MESH
BF = jnp.bfloat16
F32 = jnp.float32


def nt(a, b):
    return lax.dot_general(a, b, (((1,), (1,)), ((), ())), preferred_element_type=F32)


def nn(a, b):
    return lax.dot_general(a, b, (((1,), (0,)), ((), ())), preferred_element_type=F32)


def far_first(k, n):
    half = lax.div(k + 1, 2)
    return jnp.where(lax.rem(k, 2) == 1, n // 2 + half, n // 2 - half)


def iota(shape, dim):
    return lax.broadcasted_iota(jnp.int32, shape, dim)


def kernel(
    res_ref,
    ck_hbm,
    cv_hbm,
    lens_ref,
    wq_ref,
    wk_ref,
    wv_ref,
    wo_ref,
    hgain_ref,
    lam_ref,
    again_ref,
    mgain_ref,
    rid_ref,
    ridt_ref,
    logits_ref,
    gate_hbm,
    up_hbm,
    down_hbm,
    cos_ref,
    sin_ref,
    out_ref,
    nk_ref,
    nv_ref,
    kbuf,
    vbuf,
    gbuf,
    ubuf,
    dbuf,
    loc_sem,
    wqkv,
    wz,
    wos,
    woz,
    woa,
    sqs,
    sqr,
    nall,
    mgs,
    mga,
    sb,
    rb,
    ebuf,
    kvs,
    kvr,
    kvo,
    hb,
    hr,
    lhs,
    ob,
    orr,
    gz_s,
    gz_r,
    gown,
    gall,
    ds,
    dr,
    xb,
    cs,
    cr,
    fs,
    fr,
    zs,
    zr,
    s_wz,
    r_wz,
    s_wo,
    r_wo,
    s_woa,
    r_woa,
    s_sq,
    r_sq,
    s_na,
    r_na,
    s_mg,
    r_mg,
    s_rb,
    r_rb,
    s_kv,
    r_kv,
    s_h,
    r_h,
    s_o,
    r_o,
    s_gz,
    r_gz,
    s_ga,
    r_ga,
    s_d,
    r_d,
    s_x,
    r_x,
    s_xc,
    r_xc,
    s_cs,
    r_cs,
    s_f,
    r_f,
    s_z,
    r_z,
):
    z = lax.axis_index("ep_0")
    x = lax.axis_index("ep_1")
    c = lax.axis_index("ep_2")
    y = lax.axis_index("tp")
    g = x * NC + c
    p = g * NY + y
    q16 = x * NY + y

    def plane_id(other):
        og = lax.div(other, NY)
        return {"ep_1": lax.div(og, NC), "ep_2": lax.rem(og, NC), "tp": lax.rem(other, NY)}

    def to(src, dst, ssem, rsem, dev):
        pltpu.make_async_remote_copy(
            src_ref=src, dst_ref=dst, send_sem=ssem, recv_sem=rsem, device_id=dev, device_id_type=MESH
        ).start()

    def drain(ref, sem):
        pltpu.make_async_copy(ref, ref, sem).wait()

    local = [
        pltpu.make_async_copy(ck_hbm, kbuf, loc_sem.at[0]),
        pltpu.make_async_copy(cv_hbm, vbuf, loc_sem.at[1]),
        pltpu.make_async_copy(gate_hbm, gbuf, loc_sem.at[2]),
        pltpu.make_async_copy(up_hbm, ubuf, loc_sem.at[3]),
        pltpu.make_async_copy(down_hbm, dbuf, loc_sem.at[4]),
    ]
    for copy in local:
        copy.start()

    barrier = pltpu.get_barrier_semaphore()

    @pl.loop(0, NZ - 1)
    def _(k):
        pl.semaphore_signal(
            barrier, inc=1, device_id={"ep_0": lax.rem(z + far_first(k, NZ), NZ)}, device_id_type=MESH
        )

    @pl.loop(1, NP)
    def _(k):
        pl.semaphore_signal(
            barrier, inc=1, device_id=plane_id(lax.rem(p + k, NP)), device_id_type=MESH
        )

    wqkv[...] = jnp.concatenate(
        [
            wq_ref[...].astype(F32),
            wk_ref[...].astype(F32),
            wv_ref[...].astype(F32),
            jnp.zeros((4, 256), F32),
        ],
        axis=0,
    ).astype(BF)
    wz[z] = wqkv[...]
    wos[...] = wo_ref[...]
    woz[z] = wo_ref[...]
    stream = res_ref[...].astype(F32)
    own_squares = jnp.broadcast_to(jnp.sum(stream * stream, axis=1, keepdims=True), (16, 128))
    sqs[...] = own_squares
    mgs[...] = jnp.broadcast_to(mgain_ref[...].astype(F32), (8, 256))

    gcol = lax.shift_right_logical(rid_ref[:, 0:1], 3)
    grow = lax.shift_right_logical(ridt_ref[0:1, :], 3)
    same = (gcol == grow).astype(jnp.int32)
    earlier_col = (iota((16, 16), 1) < iota((16, 16), 0)).astype(jnp.int32)
    earlier_row = (iota((16, 16), 0) < iota((16, 16), 1)).astype(jnp.int32)
    rank_col = jnp.sum((same * earlier_col).astype(F32), axis=1, keepdims=True).astype(jnp.int32)
    rank_row = jnp.sum((same * earlier_row).astype(F32), axis=0, keepdims=True).astype(jnp.int32)
    dispatch = (iota((32, 16), 0) == grow * SLOTS + rank_row).astype(F32)
    combine = (iota((16, 32), 1) == gcol * SLOTS + rank_col).astype(F32)
    logits = logits_ref[...]
    exps = jnp.exp(logits - jnp.max(logits, axis=1, keepdims=True))
    gates = exps / jnp.sum(exps, axis=1, keepdims=True)
    members = jnp.zeros((16, 128), F32)
    for k in range(CHOSEN):
        member = jnp.bitwise_and(rid_ref[:, k : k + 1], GROUP_SIZE - 1)
        members = members + jnp.where(iota((16, 128), 1) == member, gates[:, k : k + 1], 0.0)
    slot_gates = lax.dot_general(
        dispatch, members, (((1,), (0,)), ((), ())), precision=lax.Precision.HIGHEST,
        preferred_element_type=F32,
    )
    for k in range(NZ):
        gz_s[k] = slot_gates[2 * k : 2 * k + 2]
    gz_r[z] = gz_s[z]

    row = iota((1024, 256), 0)
    col = iota((1024, 256), 1)
    src_g = lax.shift_right_logical(row, 7)
    src_z = jnp.bitwise_and(lax.shift_right_logical(row, 4), 7)
    src_r = jnp.bitwise_and(row, 15)
    to_query = jnp.logical_and(src_r < 8, jnp.bitwise_and(col, 63) == src_g * 8 + src_r)
    ebuf[:, 0:256] = jnp.where(to_query, 1.0, 0.0).astype(BF)
    spot = src_z * 16 + src_g * 2
    to_key = jnp.logical_and(
        jnp.logical_and(src_r >= 8, src_r < 10), col == spot + src_r - 8
    )
    to_value = jnp.logical_and(
        jnp.logical_and(src_r >= 10, src_r < 12), col == 128 + spot + src_r - 10
    )
    ebuf[:, 256:512] = jnp.where(jnp.logical_or(to_key, to_value), 1.0, 0.0).astype(BF)

    pl.semaphore_wait(barrier, NZ - 1 + NP - 1)

    @pl.loop(1, NY)
    def _(k):
        dev = {"tp": lax.rem(y + k, NY)}
        to(sqs, sqr.at[y], s_sq, r_sq, dev)
        to(mgs, mga.at[y], s_mg, r_mg, dev)

    @pl.loop(0, NZ - 1)
    def _(k):
        to(wqkv, wz.at[z], s_wz, r_wz, {"ep_0": lax.rem(z + far_first(k, NZ), NZ)})

    @pl.loop(0, NZ - 1)
    def _(k):
        dest = lax.rem(z + far_first(k, NZ), NZ)
        to(wos, woz.at[z], s_wo, r_wo, {"ep_0": dest})
        to(gz_s.at[dest], gz_r.at[z], s_gz, r_gz, {"ep_0": dest})

    sqr[y] = own_squares
    mga[y] = mgs[...]
    drain(sqr.at[pl.ds(0, NY - 1)], r_sq)
    squares = sqr[0] + sqr[1] + sqr[2] + sqr[3]
    scale = lax.rsqrt(squares[:, 0:1] / WIDTH + norm_eps)
    normed = (stream * scale * again_ref[...].astype(F32)).astype(BF)
    nall[g] = normed

    @pl.loop(1, NG)
    def _(k):
        other = lax.rem(g + k, NG)
        to(
            nall.at[g], nall.at[g], s_na, r_na,
            {"ep_1": lax.div(other, NC), "ep_2": lax.rem(other, NC)},
        )

    drain(nall.at[pl.ds(0, NG - 1)], r_na)
    drain(wz.at[pl.ds(0, NZ - 1)], r_wz)
    partial = nt(nall[...].reshape(128, 256), wz[...].reshape(256, 256))
    for k in range(NP):
        sb[k, 0:4, :] = partial[4 * k : 4 * k + 4, 0:128]
        sb[k, 4:8, :] = partial[4 * k : 4 * k + 4, 128:256]

    @pl.loop(1, NP)
    def _(k):
        other = lax.rem(p + k, NP)
        to(sb.at[other], rb.at[p], s_rb, r_rb, plane_id(other))

    rb[p] = sb[p]

    drain(woz.at[pl.ds(0, NZ - 1)], r_wo)
    drain(gz_r.at[pl.ds(0, NZ - 1)], r_gz)
    for k in range(NZ):
        gown[2 * k : 2 * k + 2, :] = gz_r[k]
    gall[g] = gown[...]
    woa[:, g] = woz[...]

    @pl.loop(1, NG)
    def _(k):
        other = lax.rem(g + k, NG)
        dev = {"ep_1": lax.div(other, NC), "ep_2": lax.rem(other, NC)}
        to(woz, woa.at[:, g], s_woa, r_woa, dev)
        to(gown, gall.at[g], s_ga, r_ga, dev)

    drain(rb.at[pl.ds(0, NP - 1)], r_rb)
    parts = rb[...].reshape(NG, NY, 8, 128)
    raw = parts[:, 0] + parts[:, 1] + parts[:, 2] + parts[:, 3]
    lane = iota((8, 128), 1)
    r_of = jnp.bitwise_and(lane, 15)
    is_query = r_of < 8
    is_key = jnp.logical_and(r_of >= 8, r_of < 10)
    low_key = jnp.bitwise_and(lane, 63) < 32
    turned = []
    for k in range(NG):
        own = raw[k]
        pair = raw[(k + NG // 2) % NG]
        if k < NG // 2:
            pair = -pair
        above = pltpu.roll(own, 96, 1)
        below = pltpu.roll(own, 32, 1)
        key_pair = jnp.where(low_key, -above, below)
        spun = own * cos_ref[k] + jnp.where(is_query, pair, key_pair) * sin_ref[k]
        turned.append(jnp.where(jnp.logical_or(is_query, is_key), spun, own))
    rows8 = jnp.concatenate([t.astype(BF) for t in turned], axis=1)
    placed = nn(rows8, ebuf[:, 256:512])
    kvs[...] = placed
    kvr[y] = placed

    @pl.loop(1, NY)
    def _(k):
        to(kvs, kvr.at[y], s_kv, r_kv, {"tp": lax.rem(y + k, NY)})

    own_keys = jnp.concatenate([placed[0:4, 0:128], placed[4:8, 0:128]], axis=1)
    own_values = jnp.concatenate([placed[0:4, 128:256], placed[4:8, 128:256]], axis=1)

    sub = iota((8, 128), 0)
    pieces = []
    for s in range(OWN):
        for m in range(2):
            keep = jnp.logical_and(
                is_query,
                lax.shift_right_logical(lane, 4) == jnp.bitwise_and(2 * sub + m, 7),
            )
            line = []
            for k in range(NG):
                low = jnp.broadcast_to(turned[k][s : s + 1, :], (8, 128))
                high = jnp.broadcast_to(turned[k][4 + s : 5 + s, :], (8, 128))
                line.append(jnp.where(keep, jnp.where(sub < 4, low, high), 0.0))
            pieces.append(jnp.concatenate(line, axis=1))
    spread = nn(jnp.concatenate(pieces, axis=0).astype(BF), ebuf[:, 0:256])
    for copy in local:
        copy.wait()
    blk = lax.shift_right_logical(iota((16, 256), 1), 6)
    row16 = iota((16, 256), 0)
    own_block = (
        lax.shift_right_logical(jnp.bitwise_and(row16, 7), 2) * 2 + lax.shift_right_logical(row16, 3)
    )
    head_low = jnp.bitwise_and(iota((16, 128), 0), 7) < 4
    lam = lam_ref[...]
    for s in range(OWN):
        queries = jnp.where(blk == own_block, spread[16 * s : 16 * s + 16], 0.0)
        scores = nt(queries.astype(BF), kbuf[s]) * 0.125
        length = lens_ref[y * OWN + s]
        scores = jnp.where(iota((16, CACHE), 1) < length, scores, masked_score)
        fresh = jnp.sum(queries * own_keys[s : s + 1], axis=1, keepdims=True) * 0.125
        top = jnp.maximum(jnp.max(scores, axis=1, keepdims=True), fresh)
        weights = jnp.exp(scores - top).astype(BF)
        fresh_weight = jnp.exp(fresh - top).astype(BF).astype(F32)
        total = jnp.sum(weights.astype(F32), axis=1, keepdims=True) + fresh_weight
        mixed = nn(weights, vbuf[s])
        values = jnp.where(
            head_low,
            mixed[:, 0:128] + fresh_weight * own_values[s : s + 1, 0:128],
            mixed[:, 128:256] + fresh_weight * own_values[s : s + 1, 128:256],
        )
        averaged = values / total
        contrast = averaged[0:8] - lam * averaged[8:16]
        contrast = (
            contrast
            * lax.rsqrt(jnp.mean(contrast * contrast, axis=1, keepdims=True) + head_eps)
            * hgain_ref[...]
        )
        rounded = contrast.astype(BF).astype(F32)
        for h in range(HEADS):
            hb[h // 2, h % 2, s : s + 1, :] = rounded[h : h + 1, :]

    hr[y] = hb[y]

    @pl.loop(1, NY)
    def _(k):
        other = lax.rem(y + k, NY)
        to(hb.at[other], hr.at[y], s_h, r_h, {"tp": other})

    drain(woa.at[:, pl.ds(0, NG - 1)], r_woa)
    drain(hr.at[pl.ds(0, NY - 1)], r_h)
    for k in range(NY):
        lhs[4 * k : 4 * k + 4, 0:128] = hr[k, 0]
        lhs[4 * k : 4 * k + 4, 128:256] = hr[k, 1]
    projected = nt(lhs[0:16].astype(BF), woa[...].reshape(WIDTH, 256))
    for k in range(NY):
        ob[k] = projected[:, 256 * k : 256 * k + 256]

    @pl.loop(1, NY)
    def _(k):
        other = lax.rem(y + k, NY)
        to(ob.at[other], orr.at[y], s_o, r_o, {"tp": other})

    orr[y] = ob[y]
    drain(orr.at[pl.ds(0, NY - 1)], r_o)
    attended = orr[0] + orr[1] + orr[2] + orr[3]
    middle = (stream + attended).astype(BF)

    routed = nn(dispatch.astype(BF), middle)
    for k in range(NZ):
        ds[k] = routed[2 * k : 2 * k + 2].astype(ds.dtype)
    dr[z] = ds[z]

    @pl.loop(0, NZ - 1)
    def _(k):
        dest = lax.rem(z + far_first(k, NZ), NZ)
        to(ds.at[dest], dr.at[z], s_d, r_d, {"ep_0": dest})

    drain(dr.at[pl.ds(0, NZ - 1)], r_d)
    for k in range(NZ):
        lhs[2 * k : 2 * k + 2, :] = dr[k].astype(F32)
    xb[x, c, y] = lhs[...].astype(BF)

    @pl.loop(1, NX * NY)
    def _(k):
        other = lax.rem(q16 + k, NX * NY)
        to(
            xb.at[x, c, y], xb.at[x, c, y], s_x, r_x.at[k],
            {"ep_1": lax.div(other, NY), "tp": lax.rem(other, NY)},
        )

    partner = {"ep_2": 1 - c}
    to(xb.at[x, c, y], xb.at[x, c, y], s_xc, r_xc, partner)

    @pl.loop(1, NX * NY)
    def _(k):
        other = lax.rem(q16 + NX * NY - k, NX * NY)
        ox, oy = lax.div(other, NY), lax.rem(other, NY)
        drain(xb.at[ox, c, oy], r_x.at[k])
        to(xb.at[ox, c, oy], xb.at[ox, c, oy], s_xc, r_xc, partner)

    drain(xb.at[:, 0], r_xc)
    drain(gall.at[pl.ds(0, NG - 1)], r_ga)
    drain(mga.at[pl.ds(0, NY - 1)], r_mg)

    wide = [xb[:, :, k].reshape(256, 256).astype(F32) for k in range(NY)]
    total_sq = jnp.zeros((256, 1), F32)
    for k in range(NY):
        total_sq = total_sq + jnp.sum(wide[k] * wide[k], axis=1, keepdims=True)
    scale = lax.rsqrt(total_sq / WIDTH + norm_eps)
    gate_act = jnp.zeros((256, 128), F32)
    up_act = jnp.zeros((256, 128), F32)
    for k in range(NY):
        mixed_in = (wide[k] * scale * mga[k, 0:1, :]).astype(BF)
        gate_act = gate_act + nn(mixed_in, gbuf[0, 256 * k : 256 * k + 256, :])
        up_act = up_act + nn(mixed_in, ubuf[0, 256 * k : 256 * k + 256, :])
    hidden = (gate_act / (1.0 + jnp.exp(-gate_act)) * up_act).astype(BF)
    slot_gate = jnp.sum(
        jnp.where(iota((256, 128), 1) == g, gall[...].reshape(256, 128), 0.0), axis=1, keepdims=True
    )
    produced = (nn(hidden, dbuf[0]) * slot_gate).reshape(NX, NC, 32, WIDTH)

    for k in range(NX):
        mine = jnp.where(c == 0, produced[k, 0], produced[k, 1])
        theirs = jnp.where(c == 0, produced[k, 1], produced[k, 0])
        for j in range(NY):
            cs[k, j] = theirs[:, 256 * j : 256 * j + 256].astype(BF)
            fs[k, j] = mine[:, 256 * j : 256 * j + 256]
    to(cs, cr, s_cs, r_cs, partner)
    drain(cr, r_cs)
    both = fs[...] + cr[...].astype(F32)
    fb = cs
    drain(cs, s_cs)
    fb[...] = both.astype(BF)

    @pl.loop(1, NX * NY)
    def _(k):
        other = lax.rem(q16 + k, NX * NY)
        ox, oy = lax.div(other, NY), lax.rem(other, NY)
        to(fb.at[ox, oy], fr.at[q16], s_f, r_f, {"ep_1": ox, "tp": oy})

    fr[q16] = fb[x, y]
    drain(fr.at[pl.ds(0, NX * NY - 1)], r_f)
    mixture = fr[0].astype(F32)
    for k in range(1, NX * NY):
        mixture = mixture + fr[k].astype(F32)
    for k in range(NZ):
        zs[k] = mixture[2 * k : 2 * k + 2].astype(zs.dtype)
    zr[z] = zs[z]

    @pl.loop(0, NZ - 1)
    def _(k):
        dest = lax.rem(z + far_first(k, NZ), NZ)
        to(zs.at[dest], zr.at[z], s_z, r_z, {"ep_0": dest})

    drain(kvr.at[pl.ds(0, NY - 1)], r_kv)
    for k in range(NY):
        for half in range(2):
            kvo[4 * k : 4 * k + 4, 128 * half : 128 * half + 128] = kvr[k, 4 * half : 4 * half + 4, 0:128]
            kvo[4 * k : 4 * k + 4, 256 + 128 * half : 384 + 128 * half] = kvr[
                k, 4 * half : 4 * half + 4, 128:256
            ]
    nk_ref[...] = kvo[:, 0:256].astype(BF)
    nv_ref[...] = kvo[:, 256:512].astype(BF)

    drain(zr.at[pl.ds(0, NZ - 1)], r_z)
    for k in range(NZ):
        lhs[2 * k : 2 * k + 2, :] = zr[k].astype(F32)
    mix = nn(combine.astype(BF), lhs[...].astype(BF))
    out_ref[...] = (middle.astype(F32) + mix).astype(BF)

    for ref, sem in (
        (wz, s_wz),
        (woz, s_wo),
        (gz_r, s_gz),
        (dr, s_d),
        (zr, s_z),
    ):
        drain(ref.at[pl.ds(0, NZ - 1)], sem)
    for ref, sem in ((sqr, s_sq), (mga, s_mg), (kvr, s_kv), (hr, s_h), (orr, s_o)):
        drain(ref.at[pl.ds(0, NY - 1)], sem)
    for ref, sem in ((nall, s_na), (gall, s_ga)):
        drain(ref.at[pl.ds(0, NG - 1)], sem)
    drain(woa.at[:, pl.ds(0, NG - 1)], s_woa)
    drain(rb.at[pl.ds(0, NP - 1)], s_rb)
    drain(fr.at[pl.ds(0, NX * NY - 1)], s_x)
    drain(fr.at[pl.ds(0, NX * NY - 1)], s_f)
    drain(xb.at[:, 0], s_xc)


def on_device(
    residual,
    cache_keys,
    cache_values,
    lengths,
    query_weight,
    key_weight,
    value_weight,
    out_weight,
    head_gain,
    mix_lambda,
    attn_gain,
    moe_gain,
    route_ids,
    route_logits,
    gate_weight,
    up_weight,
    down_weight,
):
    y = lax.axis_index("tp")
    half_dim = HEAD_DIM // 2
    inverse = rotary_base ** (-jnp.arange(half_dim, dtype=F32) / half_dim)
    gg = jnp.arange(NG)[:, None]
    lane = jnp.arange(128)[None, :]
    r_of = lane % 16
    at_query = (gg % (NG // 2)) * 8 + r_of % 8
    at_key = ((lane // 16) % 2) * 16 + gg * 2 + r_of % 2
    entry = jnp.where(r_of < 8, at_query, at_key)
    table = inverse[entry]
    own = lax.dynamic_slice_in_dim(lengths, y * OWN, OWN, 0).astype(F32)
    rows = jnp.concatenate([own, own])
    angles = rows[None, :, None] * table[:, None, :]
    cosine, sine = jnp.cos(angles), jnp.sin(angles)

    vm = pl.BlockSpec(memory_space=pltpu.VMEM)
    hbm = pl.BlockSpec(memory_space=pl.ANY)
    smem = pl.BlockSpec(memory_space=pltpu.SMEM)
    dma = pltpu.SemaphoreType.DMA
    V = pltpu.VMEM
    scratch = [
        V((OWN, CACHE, 256), BF),
        V((OWN, CACHE, 256), BF),
        V((1, WIDTH, 128), BF),
        V((1, WIDTH, 128), BF),
        V((1, 128, WIDTH), BF),
        dma((5,)),
        V((16, 256), BF),
        V((NZ, 16, 256), BF),
        V((8, 256), BF),
        V((NZ, 8, 256), BF),
        V((NZ, NG, 8, 256), BF),
        V((16, 128), F32),
        V((NY, 16, 128), F32),
        V((NG, 16, 256), BF),
        V((8, 256), F32),
        V((NY, 8, 256), F32),
        V((NP, 8, 128), F32),
        V((NP, 8, 128), F32),
        V((1024, 512), BF),
        V((8, 256), F32),
        V((NY, 8, 256), F32),
        V((16, 512), F32),
        V((NY, 2, OWN, 128), F32),
        V((NY, 2, OWN, 128), F32),
        V((32, 256), F32),
        V((NY, 16, 256), F32),
        V((NY, 16, 256), F32),
        V((NZ, SLOTS, 128), F32),
        V((NZ, SLOTS, 128), F32),
        V((32, 128), F32),
        V((NG, 32, 128), F32),
        V((NZ, SLOTS, 256), F32),
        V((NZ, SLOTS, 256), F32),
        V((NX, NC, NY, 32, 256), BF),
        V((NX, NY, 32, 256), BF),
        V((NX, NY, 32, 256), BF),
        V((NX, NY, 32, 256), F32),
        V((NX * NY, 32, 256), BF),
        V((NZ, SLOTS, 256), F32),
        V((NZ, SLOTS, 256), F32),
    ]
    sems = [dma] * 36
    sems[27] = dma((NX * NY,))
    out, nk, nv = pl.pallas_call(
        kernel,
        out_shape=(
            jax.ShapeDtypeStruct((16, 256), BF),
            jax.ShapeDtypeStruct((16, 256), BF),
            jax.ShapeDtypeStruct((16, 256), BF),
        ),
        in_specs=[vm, hbm, hbm, smem] + [vm] * 11 + [hbm] * 3 + [vm] * 2,
        out_specs=(vm, vm, vm),
        scratch_shapes=scratch + sems,
        compiler_params=pltpu.CompilerParams(
            collective_id=0, has_side_effects=True, vmem_limit_bytes=40 * 2**20
        ),
        cost_estimate=pl.CostEstimate(flops=10**9, bytes_accessed=5 * 10**6, transcendentals=0),
    )(
        residual,
        cache_keys,
        cache_values,
        lengths,
        query_weight.T,
        key_weight.T,
        value_weight.T,
        out_weight.T,
        head_gain.reshape(1, 128),
        mix_lambda.reshape(HEADS, 1),
        attn_gain.reshape(1, 256),
        moe_gain.reshape(1, 256),
        route_ids,
        route_ids.T,
        route_logits,
        gate_weight,
        up_weight,
        down_weight,
        cosine,
        sine,
    )
    return out, nk, nv


def solution(mesh):
    torus = Mesh(mesh.devices.reshape(NZ, NX, NC, NY), ("ep_0", "ep_1", "ep_2", "tp"))
    return jax.shard_map(
        on_device,
        mesh=torus,
        in_specs=(
            P(EP, "tp"),
            P(EP_TP, None, None),
            P(EP_TP, None, None),
            P(EP),
            P("tp", EP),
            P("tp", EP),
            P("tp", EP),
            P("tp", EP),
            P(),
            P(),
            P("tp"),
            P("tp"),
            P(EP, None),
            P(EP, None),
            P(EP, None, "tp"),
            P(EP, None, "tp"),
            P(EP, "tp", None),
        ),
        out_specs=(P(EP, "tp"), P(EP, None), P(EP, None)),
        check_vma=False,
    )
```

time: 261 us -> 85.1 us (0.33)
  blocking collectives: 114 us -> 0 us
  Pallas kernels: 0 us -> 71.2 us
  waiting for transfers between devices: 57.3 us -> 0 us
  starting transfers between devices: 42.7 us -> 0 us
  between operations: 14.5 us -> 0.86 us
  local copies, waits for them, and re-layouts: 22.6 us -> 11.6 us
  matrix products: 6.02 us -> 0 us
    all_gather x7 -> x0, blocking collectives: 98.4 us -> none  [the longest x6 88.9 us: all_blocks(): tiles = lax.all_gather(tiles, axes[k])]
    pallas_call x0 -> x1, Pallas kernels: none -> 71.2 us  [on_device(): pl.pallas_call(kernel, out_shape=(jax.ShapeDtypeStruct((16, 256), BF), ja...]
    all_to_all x5 -> x0, waiting for transfers between devices: 47.4 us -> none  [the longest x2 17.3 us: sum_at_owner(): lax.all_to_all(tiles, axis, split_axis=0, concat_axis=0, tiled=True)]
    all_to_all x5 -> x0, starting transfers between devices: 42.7 us -> none  [the longest x1 21.3 us: on_device(): lax.all_to_all(outgoing, EP, split_axis=0, concat_axis=0, tiled=True)]
    psum x2 -> x0, blocking collectives: 15.6 us -> none  [the longest x1 8.72 us: on_device(): squares = lax.psum(jnp.sum(stream * stream, axis=1), 'tp')]
    psum x1 -> x0, waiting for transfers between devices: 9.88 us -> none  [on_device(): projected = lax.psum(partial_cols, 'tp')]
    gather x0 -> x1, local copies, waits for them, and re-layouts: none -> 6.57 us  [on_device(): table = inverse[entry]]
    reshape x8 -> x3, local copies, waits for them, and re-layouts: 7.52 us -> 1.4 us  [the longest x1 0.66 us: on_device(): attn_gain.reshape(1, 256)]
  transfers between devices with their start and end apart: 6 -> 0, of which waited for: 5 -> 0; matrix products, arithmetic and copies ran while one was open for 4% -> 0% of each run, Pallas kernels for 0% -> 0%
where the time goes in v1:
time: 85.1 us; the launch traced here: 84.8 us
  Pallas kernels  71.2 us (84%)
  local copies, waits for them, and re-layouts  11.6 us (14%)
  other arithmetic  1.12 us (1%)
  between operations  0.86 us (1%)
    pallas_call x1, Pallas kernels, on_device(): pl.pallas_call(kernel, out_shape=(jax.ShapeDtypeStruct((16, 256), BF), ja...  71.2 us
    gather x1, local copies, waits for them, and re-layouts, on_device(): table = inverse[entry]  6.57 us
    unnamed x35, local copies, waits for them, and re-layouts  3.63 us

profile of v1, /device:TPU:1, one launch (start us, length us, event | category | flops | bytes accessed | tf_op | source)
XLA Modules:
  0.0 84.8 jit_solution(6529718128019865042)
XLA Ops:
  0.6 0.7 dynamic-slice_convert_fusion
  1.4 0.1 pad_maximum_fusion
  1.5 0.7 reshape.292.again_ref
  2.1 0.7 reshape.293.mgain_ref
  2.8 0.1 fusion.1
  2.9 0.0 copy-start.14
  2.9 0.0 copy-start.13
  2.9 0.0 copy-start.5
  2.9 0.0 copy-start
  2.9 0.0 copy-start.2
  2.9 0.0 copy-start.3
  2.9 0.0 copy-start.4
  2.9 0.0 copy-start.6
  3.0 0.0 copy-start.7
  3.0 0.0 copy-start.8
  3.0 0.0 copy-start.9
  3.0 0.0 copy-start.10
  3.0 0.0 copy-start.11
  3.0 0.0 copy-start.12
  3.0 6.6 %gather_fusion = f32[1024]{0:T(1024)S(1)} fusion(f32[32]{0:T(128)S(1)} %multiply_power_fusion, s32[1024]{0:T(1024)S(1)} %fusion.1), kind=kCustom, calls=%fused_computation | custom fusion | bytes 12288 | tf_op jit(solution)/shard_map/gather | solution.py:573
  9.6 0.0 copy-done.14
  9.6 0.1 copy.23.lam_ref
  9.7 0.0 copy-done.13
  9.7 0.1 copy.25.logits_ref
  9.8 0.0 copy-done.5
  9.8 0.1 copy.24.rid_ref
  9.9 0.2 multiply_sine_fusion
  10.1 0.0 copy-done
  10.1 0.0 copy-done.2
  10.1 0.0 copy-done.3
  10.1 0.0 copy-done.4
  10.1 0.0 copy-done.6
  10.1 0.0 copy-done.7
  10.1 0.0 copy-done.8
  10.1 0.0 copy-done.9
  10.2 0.0 copy-done.10
  10.2 0.0 copy-done.11
  10.2 0.0 copy-done.12
  10.2 0.0 copy-start.1
  10.2 1.6 %copy-done.1 = bf16[4,1024,256]{2,1,0:T(8,128)(2,1)S(1)} copy-done((bf16[4,1024,256]{2,1,0:T(8,128)(2,1)S(1)}, bf16[4,1024,256]{2,1,0:T(8,128)(2,1)}, u32[]{:S(2)}) %copy-start.1) | copy-done | bytes 2097176
  11.8 71.2 %shard_map.184 = (bf16[16,256]{1,0:T(8,128)(2,1)S(1)}, bf16[16,256]{1,0:T(8,128)(2,1)S(1)}, bf16[16,256]{1,0:T(8,128)(2,1)S(1)}) custom-call(bf16[16,256]{1,0:T(8,128)(2,1)S(1)} %copy-done.6, bf16[4,1024,256]{2,1,0:T(8,128)(2,1)S(1)} %copy-done, bf16[4,1024,256]{2,1,0:T(8,128)(2,1)S(1)} %copy-done.1, s32[16]{0:T(128)S(1)} %copy-done.11, ...), custom_call_target="tpu_custom_call" | custom-call | flops 1000000000 | bytes 5000000 | tf_op jit(solution)/shard_map/pallas_call | solution.py:628
  83.0 0.6 copy.29
  83.6 0.6 copy.30
  84.2 0.6 copy.31
  (5 shorter events, 0.0 us)
Async XLA Ops:
  2.9 6.7 %copy-start.14 = (f32[8]{0:T(128)S(1)}, f32[8]{0:T(128)}, u32[]{:S(2)}) copy-start(f32[8]{0:T(128)} %param.26) | copy-start | bytes 100
  2.9 6.8 %copy-start.13 = (f32[16,6]{0,1:T(8,128)S(1)}, f32[16,6]{0,1:T(8,128)}, u32[]{:S(2)}) copy-start(f32[16,6]{0,1:T(8,128)} %param.30) | copy-start | bytes 1156
  2.9 6.9 %copy-start.5 = (s32[16,6]{0,1:T(8,128)S(1)}, s32[16,6]{0,1:T(8,128)}, u32[]{:S(2)}) copy-start(s32[16,6]{0,1:T(8,128)} %param.29) | copy-start | bytes 1156
  2.9 7.2 %copy-start = (bf16[4,1024,256]{2,1,0:T(8,128)(2,1)S(1)}, bf16[4,1024,256]{2,1,0:T(8,128)(2,1)}, u32[]{:S(2)}) copy-start(bf16[4,1024,256]{2,1,0:T(8,128)(2,1)} %ck_hbm.1) | copy-start | bytes 6291460
  2.9 7.2 %copy-start.2 = (bf16[1,1024,128]{2,1,0:T(8,128)(2,1)S(1)}, bf16[1,1024,128]{2,1,0:T(8,128)(2,1)}, u32[]{:S(2)}) copy-start(bf16[1,1024,128]{2,1,0:T(8,128)(2,1)} %gate_hbm.1) | copy-start | bytes 786436
  2.9 7.2 %copy-start.3 = (bf16[1,1024,128]{2,1,0:T(8,128)(2,1)S(1)}, bf16[1,1024,128]{2,1,0:T(8,128)(2,1)}, u32[]{:S(2)}) copy-start(bf16[1,1024,128]{2,1,0:T(8,128)(2,1)} %up_hbm.1) | copy-start | bytes 786436
  2.9 7.2 %copy-start.4 = (bf16[1,128,1024]{2,1,0:T(8,128)(2,1)S(1)}, bf16[1,128,1024]{2,1,0:T(8,128)(2,1)}, u32[]{:S(2)}) copy-start(bf16[1,128,1024]{2,1,0:T(8,128)(2,1)} %down_hbm.1) | copy-start | bytes 786436
  2.9 7.2 %copy-start.6 = (bf16[16,256]{1,0:T(8,128)(2,1)S(1)}, bf16[16,256]{1,0:T(8,128)(2,1)}, u32[]{:S(2)}) copy-start(bf16[16,256]{1,0:T(8,128)(2,1)} %res_ref.1) | copy-start | bytes 24580
  3.0 7.2 %copy-start.7 = (bf16[256,8]{0,1:T(8,128)(2,1)S(1)}, bf16[256,8]{0,1:T(8,128)(2,1)}, u32[]{:S(2)}) copy-start(bf16[256,8]{0,1:T(8,128)(2,1)} %param.21) | copy-start | bytes 12292
  3.0 7.2 %copy-start.8 = (bf16[256,8]{0,1:T(8,128)(2,1)S(1)}, bf16[256,8]{0,1:T(8,128)(2,1)}, u32[]{:S(2)}) copy-start(bf16[256,8]{0,1:T(8,128)(2,1)} %param.24) | copy-start | bytes 12292
  3.0 7.2 %copy-start.9 = (bf16[256,2]{0,1:T(2,128)(2,1)S(1)}, bf16[256,2]{0,1:T(2,128)(2,1)}, u32[]{:S(2)}) copy-start(bf16[256,2]{0,1:T(2,128)(2,1)} %param.22) | copy-start | bytes 3076
  3.0 7.2 %copy-start.10 = (bf16[256,2]{0,1:T(2,128)(2,1)S(1)}, bf16[256,2]{0,1:T(2,128)(2,1)}, u32[]{:S(2)}) copy-start(bf16[256,2]{0,1:T(2,128)(2,1)} %param.23) | copy-start | bytes 3076
  3.0 7.2 %copy-start.11 = (s32[16]{0:T(128)S(1)}, s32[16]{0:T(128)}, u32[]{:S(2)}) copy-start(s32[16]{0:T(128)} %lens_ref.1) | copy-start | bytes 196
  3.0 7.2 %copy-start.12 = (f32[128]{0:T(128)S(1)}, f32[128]{0:T(128)}, u32[]{:S(2)}) copy-start(f32[128]{0:T(128)} %param.25) | copy-start | bytes 1540
  10.2 1.6 %copy-start.1 = (bf16[4,1024,256]{2,1,0:T(8,128)(2,1)S(1)}, bf16[4,1024,256]{2,1,0:T(8,128)(2,1)}, u32[]{:S(2)}) copy-start(bf16[4,1024,256]{2,1,0:T(8,128)(2,1)} %cv_hbm.1) | copy-start | bytes 6291460

commit v2 on v1

--- a/solution.py
+++ b/solution.py
@@ -1,3 +1,5 @@
+import math
+
 import jax
 import jax.numpy as jnp
 from jax import lax
@@ -49,9 +51,25 @@
 
 
 def kernel(
-    res_ref,
+    res_hbm,
     ck_hbm,
     cv_hbm,
+    lens_hbm,
+    wq_hbm,
+    wk_hbm,
+    wv_hbm,
+    wo_hbm,
+    hgain_hbm,
+    lam_hbm,
+    again_hbm,
+    mgain_hbm,
+    ridt_hbm,
+    logitst_hbm,
+    gate_hbm,
+    up_hbm,
+    down_hbm,
+    out_ref,
+    res_ref,
     lens_ref,
     wq_ref,
     wk_ref,
@@ -61,17 +79,8 @@
     lam_ref,
     again_ref,
     mgain_ref,
-    rid_ref,
     ridt_ref,
-    logits_ref,
-    gate_hbm,
-    up_hbm,
-    down_hbm,
-    cos_ref,
-    sin_ref,
-    out_ref,
-    nk_ref,
-    nv_ref,
+    logitst_ref,
     kbuf,
     vbuf,
     gbuf,
@@ -91,6 +100,8 @@
     sb,
     rb,
     ebuf,
+    cosb,
+    sinb,
     kvs,
     kvr,
     kvo,
@@ -106,8 +117,6 @@
     ds,
     dr,
     xb,
-    cs,
-    cr,
     fs,
     fr,
     zs,
@@ -140,10 +149,8 @@
     r_d,
     s_x,
     r_x,
-    s_xc,
-    r_xc,
-    s_cs,
-    r_cs,
+    s_ew,
+    r_ew,
     s_f,
     r_f,
     s_z,
@@ -169,16 +176,6 @@
     def drain(ref, sem):
         pltpu.make_async_copy(ref, ref, sem).wait()
 
-    local = [
-        pltpu.make_async_copy(ck_hbm, kbuf, loc_sem.at[0]),
-        pltpu.make_async_copy(cv_hbm, vbuf, loc_sem.at[1]),
-        pltpu.make_async_copy(gate_hbm, gbuf, loc_sem.at[2]),
-        pltpu.make_async_copy(up_hbm, ubuf, loc_sem.at[3]),
-        pltpu.make_async_copy(down_hbm, dbuf, loc_sem.at[4]),
-    ]
-    for copy in local:
-        copy.start()
-
     barrier = pltpu.get_barrier_semaphore()
 
     @pl.loop(0, NZ - 1)
@@ -193,6 +190,38 @@
             barrier, inc=1, device_id=plane_id(lax.rem(p + k, NP)), device_id_type=MESH
         )
 
+    small = [
+        pltpu.make_async_copy(src, dst, loc_sem.at[k])
+        for k, (src, dst) in enumerate(
+            (
+                (res_hbm, res_ref),
+                (wq_hbm, wq_ref),
+                (wk_hbm, wk_ref),
+                (wv_hbm, wv_ref),
+                (wo_hbm, wo_ref),
+                (mgain_hbm, mgain_ref),
+                (again_hbm, again_ref),
+                (hgain_hbm, hgain_ref),
+                (ridt_hbm, ridt_ref),
+                (logitst_hbm, logitst_ref),
+                (lens_hbm, lens_ref),
+                (lam_hbm, lam_ref),
+            )
+        )
+    ]
+    experts = [
+        pltpu.make_async_copy(gate_hbm.at[0], gbuf.at[c], loc_sem.at[12]),
+        pltpu.make_async_copy(up_hbm.at[0], ubuf.at[c], loc_sem.at[13]),
+        pltpu.make_async_copy(down_hbm.at[0], dbuf.at[c], loc_sem.at[14]),
+    ]
+    caches = [
+        pltpu.make_async_copy(ck_hbm, kbuf, loc_sem.at[15]),
+        pltpu.make_async_copy(cv_hbm, vbuf, loc_sem.at[16]),
+    ]
+    for copy in small + experts + caches:
+        copy.start()
+    for copy in small:
+        copy.wait()
     wqkv[...] = jnp.concatenate(
         [
             wq_ref[...].astype(F32),
@@ -208,26 +237,26 @@
     stream = res_ref[...].astype(F32)
     own_squares = jnp.broadcast_to(jnp.sum(stream * stream, axis=1, keepdims=True), (16, 128))
     sqs[...] = own_squares
-    mgs[...] = jnp.broadcast_to(mgain_ref[...].astype(F32), (8, 256))
-
-    gcol = lax.shift_right_logical(rid_ref[:, 0:1], 3)
-    grow = lax.shift_right_logical(ridt_ref[0:1, :], 3)
-    same = (gcol == grow).astype(jnp.int32)
-    earlier_col = (iota((16, 16), 1) < iota((16, 16), 0)).astype(jnp.int32)
-    earlier_row = (iota((16, 16), 0) < iota((16, 16), 1)).astype(jnp.int32)
-    rank_col = jnp.sum((same * earlier_col).astype(F32), axis=1, keepdims=True).astype(jnp.int32)
-    rank_row = jnp.sum((same * earlier_row).astype(F32), axis=0, keepdims=True).astype(jnp.int32)
-    dispatch = (iota((32, 16), 0) == grow * SLOTS + rank_row).astype(F32)
-    combine = (iota((16, 32), 1) == gcol * SLOTS + rank_col).astype(F32)
-    logits = logits_ref[...]
-    exps = jnp.exp(logits - jnp.max(logits, axis=1, keepdims=True))
-    gates = exps / jnp.sum(exps, axis=1, keepdims=True)
-    members = jnp.zeros((16, 128), F32)
+    mgs[...] = jnp.broadcast_to(mgain_ref[...].astype(F32).reshape(1, 256), (8, 256))
+
+    groups = lax.shift_right_logical(ridt_ref[0:1, :], 3).astype(F32)
+    grow = jnp.broadcast_to(groups, (16, 16))
+    eye = (iota((16, 16), 0) == iota((16, 16), 1)).astype(F32)
+    gcol = nt(eye, grow)
+    before = jnp.logical_and(grow == gcol, iota((16, 16), 0) < iota((16, 16), 1))
+    rank = jnp.sum(jnp.where(before, 1.0, 0.0), axis=0, keepdims=True)
+    slot = groups * SLOTS + rank
+    dispatch = jnp.where(iota((32, 16), 0).astype(F32) == slot, 1.0, 0.0)
+    combine = nt(eye, dispatch)
+    logits = logitst_ref[...]
+    exps = jnp.exp(logits - jnp.max(logits, axis=0, keepdims=True))
+    gates = exps / jnp.sum(exps, axis=0, keepdims=True)
+    members = jnp.zeros((128, 16), F32)
     for k in range(CHOSEN):
-        member = jnp.bitwise_and(rid_ref[:, k : k + 1], GROUP_SIZE - 1)
-        members = members + jnp.where(iota((16, 128), 1) == member, gates[:, k : k + 1], 0.0)
+        member = jnp.bitwise_and(ridt_ref[k : k + 1, :], GROUP_SIZE - 1)
+        members = members + jnp.where(iota((128, 16), 0) == member, gates[k : k + 1, :], 0.0)
     slot_gates = lax.dot_general(
-        dispatch, members, (((1,), (0,)), ((), ())), precision=lax.Precision.HIGHEST,
+        dispatch, members, (((1,), (1,)), ((), ())), precision=lax.Precision.HIGHEST,
         preferred_element_type=F32,
     )
     for k in range(NZ):
@@ -250,6 +279,24 @@
     )
     ebuf[:, 256:512] = jnp.where(jnp.logical_or(to_key, to_value), 1.0, 0.0).astype(BF)
 
+    lane = iota((8, 128), 1)
+    sub = iota((8, 128), 0)
+    r_of = jnp.bitwise_and(lane, 15)
+    place = jnp.zeros((8, 128), F32)
+    for s in range(OWN):
+        place = jnp.where(
+            jnp.bitwise_and(sub, 3) == s, lens_ref[y * OWN + s].astype(F32), place
+        )
+    for k in range(NG):
+        at_query = (k % (NG // 2)) * 8 + jnp.bitwise_and(r_of, 7)
+        at_key = jnp.bitwise_and(lax.shift_right_logical(lane, 4), 1) * 16 + k * 2 + (
+            jnp.bitwise_and(r_of, 1)
+        )
+        entry = jnp.where(r_of < 8, at_query, at_key).astype(F32)
+        angle = place * jnp.exp(entry * (-math.log(rotary_base) / (HEAD_DIM // 2)))
+        cosb[k] = jnp.cos(angle)
+        sinb[k] = jnp.sin(angle)
+
     pl.semaphore_wait(barrier, NZ - 1 + NP - 1)
 
     @pl.loop(1, NY)
@@ -261,19 +308,13 @@
     @pl.loop(0, NZ - 1)
     def _(k):
         to(wqkv, wz.at[z], s_wz, r_wz, {"ep_0": lax.rem(z + far_first(k, NZ), NZ)})
-
-    @pl.loop(0, NZ - 1)
-    def _(k):
-        dest = lax.rem(z + far_first(k, NZ), NZ)
-        to(wos, woz.at[z], s_wo, r_wo, {"ep_0": dest})
-        to(gz_s.at[dest], gz_r.at[z], s_gz, r_gz, {"ep_0": dest})
 
     sqr[y] = own_squares
     mga[y] = mgs[...]
     drain(sqr.at[pl.ds(0, NY - 1)], r_sq)
     squares = sqr[0] + sqr[1] + sqr[2] + sqr[3]
     scale = lax.rsqrt(squares[:, 0:1] / WIDTH + norm_eps)
-    normed = (stream * scale * again_ref[...].astype(F32)).astype(BF)
+    normed = (stream * scale * again_ref[...].astype(F32).reshape(1, 256)).astype(BF)
     nall[g] = normed
 
     @pl.loop(1, NG)
@@ -283,6 +324,17 @@
             nall.at[g], nall.at[g], s_na, r_na,
             {"ep_1": lax.div(other, NC), "ep_2": lax.rem(other, NC)},
         )
+
+    @pl.loop(0, NZ - 1)
+    def _(k):
+        dest = lax.rem(z + far_first(k, NZ), NZ)
+        to(wos, woz.at[z], s_wo, r_wo, {"ep_0": dest})
+        to(gz_s.at[dest], gz_r.at[z], s_gz, r_gz, {"ep_0": dest})
+
+    partner = {"ep_2": 1 - c}
+    for k, ref in enumerate((gbuf, ubuf, dbuf)):
+        experts[k].wait()
+        to(ref.at[c], ref.at[c], s_ew.at[k], r_ew.at[k], partner)
 
     drain(nall.at[pl.ds(0, NG - 1)], r_na)
     drain(wz.at[pl.ds(0, NZ - 1)], r_wz)
@@ -302,7 +354,7 @@
     drain(gz_r.at[pl.ds(0, NZ - 1)], r_gz)
     for k in range(NZ):
         gown[2 * k : 2 * k + 2, :] = gz_r[k]
-    gall[g] = gown[...]
+    gall[x] = gown[...]
     woa[:, g] = woz[...]
 
     @pl.loop(1, NG)
@@ -310,13 +362,14 @@
         other = lax.rem(g + k, NG)
         dev = {"ep_1": lax.div(other, NC), "ep_2": lax.rem(other, NC)}
         to(woz, woa.at[:, g], s_woa, r_woa, dev)
-        to(gown, gall.at[g], s_ga, r_ga, dev)
+
+    @pl.loop(1, NX)
+    def _(k):
+        to(gown, gall.at[x], s_ga, r_ga, {"ep_1": lax.rem(x + k, NX)})
 
     drain(rb.at[pl.ds(0, NP - 1)], r_rb)
     parts = rb[...].reshape(NG, NY, 8, 128)
     raw = parts[:, 0] + parts[:, 1] + parts[:, 2] + parts[:, 3]
-    lane = iota((8, 128), 1)
-    r_of = jnp.bitwise_and(lane, 15)
     is_query = r_of < 8
     is_key = jnp.logical_and(r_of >= 8, r_of < 10)
     low_key = jnp.bitwise_and(lane, 63) < 32
@@ -329,7 +382,7 @@
         above = pltpu.roll(own, 96, 1)
         below = pltpu.roll(own, 32, 1)
         key_pair = jnp.where(low_key, -above, below)
-        spun = own * cos_ref[k] + jnp.where(is_query, pair, key_pair) * sin_ref[k]
+        spun = own * cosb[k] + jnp.where(is_query, pair, key_pair) * sinb[k]
         turned.append(jnp.where(jnp.logical_or(is_query, is_key), spun, own))
     rows8 = jnp.concatenate([t.astype(BF) for t in turned], axis=1)
     placed = nn(rows8, ebuf[:, 256:512])
@@ -343,7 +396,6 @@
     own_keys = jnp.concatenate([placed[0:4, 0:128], placed[4:8, 0:128]], axis=1)
     own_values = jnp.concatenate([placed[0:4, 128:256], placed[4:8, 128:256]], axis=1)
 
-    sub = iota((8, 128), 0)
     pieces = []
     for s in range(OWN):
         for m in range(2):
@@ -358,7 +410,7 @@
                 line.append(jnp.where(keep, jnp.where(sub < 4, low, high), 0.0))
             pieces.append(jnp.concatenate(line, axis=1))
     spread = nn(jnp.concatenate(pieces, axis=0).astype(BF), ebuf[:, 0:256])
-    for copy in local:
+    for copy in caches:
         copy.wait()
     blk = lax.shift_right_logical(iota((16, 256), 1), 6)
     row16 = iota((16, 256), 0)
@@ -366,7 +418,9 @@
         lax.shift_right_logical(jnp.bitwise_and(row16, 7), 2) * 2 + lax.shift_right_logical(row16, 3)
     )
     head_low = jnp.bitwise_and(iota((16, 128), 0), 7) < 4
-    lam = lam_ref[...]
+    lam = jnp.zeros((8, 128), F32)
+    for h in range(HEADS):
+        lam = jnp.where(sub == h, lam_ref[h], lam)
     for s in range(OWN):
         queries = jnp.where(blk == own_block, spread[16 * s : 16 * s + 16], 0.0)
         scores = nt(queries.astype(BF), kbuf[s]) * 0.125
@@ -388,7 +442,7 @@
         contrast = (
             contrast
             * lax.rsqrt(jnp.mean(contrast * contrast, axis=1, keepdims=True) + head_eps)
-            * hgain_ref[...]
+            * hgain_ref[...].reshape(1, 128)
         )
         rounded = contrast.astype(BF).astype(F32)
         for h in range(HEADS):
@@ -433,67 +487,55 @@
     drain(dr.at[pl.ds(0, NZ - 1)], r_d)
     for k in range(NZ):
         lhs[2 * k : 2 * k + 2, :] = dr[k].astype(F32)
-    xb[x, c, y] = lhs[...].astype(BF)
+    xb[x, y] = lhs[...].astype(BF)
 
     @pl.loop(1, NX * NY)
     def _(k):
         other = lax.rem(q16 + k, NX * NY)
         to(
-            xb.at[x, c, y], xb.at[x, c, y], s_x, r_x.at[k],
+            xb.at[x, y], xb.at[x, y], s_x, r_x,
             {"ep_1": lax.div(other, NY), "tp": lax.rem(other, NY)},
         )
 
-    partner = {"ep_2": 1 - c}
-    to(xb.at[x, c, y], xb.at[x, c, y], s_xc, r_xc, partner)
-
-    @pl.loop(1, NX * NY)
-    def _(k):
-        other = lax.rem(q16 + NX * NY - k, NX * NY)
-        ox, oy = lax.div(other, NY), lax.rem(other, NY)
-        drain(xb.at[ox, c, oy], r_x.at[k])
-        to(xb.at[ox, c, oy], xb.at[ox, c, oy], s_xc, r_xc, partner)
-
-    drain(xb.at[:, 0], r_xc)
-    drain(gall.at[pl.ds(0, NG - 1)], r_ga)
+    drain(gall.at[pl.ds(0, NX - 1)], r_ga)
     drain(mga.at[pl.ds(0, NY - 1)], r_mg)
-
-    wide = [xb[:, :, k].reshape(256, 256).astype(F32) for k in range(NY)]
-    total_sq = jnp.zeros((256, 1), F32)
+    for k, ref in enumerate((gbuf, ubuf, dbuf)):
+        drain(ref.at[0], r_ew.at[k])
+    drain(fr.at[pl.ds(0, NX * NY - 1)], r_x)
+
+    rows = NX * 32
+    wide = [xb[:, k].reshape(rows, 256).astype(F32) for k in range(NY)]
+    total_sq = jnp.zeros((rows, 1), F32)
     for k in range(NY):
         total_sq = total_sq + jnp.sum(wide[k] * wide[k], axis=1, keepdims=True)
     scale = lax.rsqrt(total_sq / WIDTH + norm_eps)
-    gate_act = jnp.zeros((256, 128), F32)
-    up_act = jnp.zeros((256, 128), F32)
-    for k in range(NY):
-        mixed_in = (wide[k] * scale * mga[k, 0:1, :]).astype(BF)
-        gate_act = gate_act + nn(mixed_in, gbuf[0, 256 * k : 256 * k + 256, :])
-        up_act = up_act + nn(mixed_in, ubuf[0, 256 * k : 256 * k + 256, :])
-    hidden = (gate_act / (1.0 + jnp.exp(-gate_act)) * up_act).astype(BF)
-    slot_gate = jnp.sum(
-        jnp.where(iota((256, 128), 1) == g, gall[...].reshape(256, 128), 0.0), axis=1, keepdims=True
-    )
-    produced = (nn(hidden, dbuf[0]) * slot_gate).reshape(NX, NC, 32, WIDTH)
+    mixed_in = [(wide[k] * scale * mga[k, 0:1, :]).astype(BF) for k in range(NY)]
+    produced = jnp.zeros((rows, WIDTH), F32)
+    for e in range(NC):
+        gate_act = jnp.zeros((rows, 128), F32)
+        up_act = jnp.zeros((rows, 128), F32)
+        for k in range(NY):
+            gate_act = gate_act + nn(mixed_in[k], gbuf[e, 256 * k : 256 * k + 256, :])
+            up_act = up_act + nn(mixed_in[k], ubuf[e, 256 * k : 256 * k + 256, :])
+        hidden = (gate_act / (1.0 + jnp.exp(-gate_act)) * up_act).astype(BF)
+        slot_gate = jnp.sum(
+            jnp.where(iota((rows, 128), 1) == x * NC + e, gall[...].reshape(rows, 128), 0.0),
+            axis=1,
+            keepdims=True,
+        )
+        produced = produced + nn(hidden, dbuf[e]) * slot_gate
 
     for k in range(NX):
-        mine = jnp.where(c == 0, produced[k, 0], produced[k, 1])
-        theirs = jnp.where(c == 0, produced[k, 1], produced[k, 0])
         for j in range(NY):
-            cs[k, j] = theirs[:, 256 * j : 256 * j + 256].astype(BF)
-            fs[k, j] = mine[:, 256 * j : 256 * j + 256]
-    to(cs, cr, s_cs, r_cs, partner)
-    drain(cr, r_cs)
-    both = fs[...] + cr[...].astype(F32)
-    fb = cs
-    drain(cs, s_cs)
-    fb[...] = both.astype(BF)
+            fs[k, j] = produced[32 * k : 32 * k + 32, 256 * j : 256 * j + 256].astype(BF)
 
     @pl.loop(1, NX * NY)
     def _(k):
         other = lax.rem(q16 + k, NX * NY)
         ox, oy = lax.div(other, NY), lax.rem(other, NY)
-        to(fb.at[ox, oy], fr.at[q16], s_f, r_f, {"ep_1": ox, "tp": oy})
-
-    fr[q16] = fb[x, y]
+        to(fs.at[ox, oy], fr.at[q16], s_f, r_f, {"ep_1": ox, "tp": oy})
+
+    fr[q16] = fs[x, y]
     drain(fr.at[pl.ds(0, NX * NY - 1)], r_f)
     mixture = fr[0].astype(F32)
     for k in range(1, NX * NY):
@@ -514,14 +556,14 @@
             kvo[4 * k : 4 * k + 4, 256 + 128 * half : 384 + 128 * half] = kvr[
                 k, 4 * half : 4 * half + 4, 128:256
             ]
-    nk_ref[...] = kvo[:, 0:256].astype(BF)
-    nv_ref[...] = kvo[:, 256:512].astype(BF)
+    out_ref[1] = kvo[:, 0:256].astype(BF)
+    out_ref[2] = kvo[:, 256:512].astype(BF)
 
     drain(zr.at[pl.ds(0, NZ - 1)], r_z)
     for k in range(NZ):
         lhs[2 * k : 2 * k + 2, :] = zr[k].astype(F32)
     mix = nn(combine.astype(BF), lhs[...].astype(BF))
-    out_ref[...] = (middle.astype(F32) + mix).astype(BF)
+    out_ref[0] = (middle.astype(F32) + mix).astype(BF)
 
     for ref, sem in (
         (wz, s_wz),
@@ -533,13 +575,14 @@
         drain(ref.at[pl.ds(0, NZ - 1)], sem)
     for ref, sem in ((sqr, s_sq), (mga, s_mg), (kvr, s_kv), (hr, s_h), (orr, s_o)):
         drain(ref.at[pl.ds(0, NY - 1)], sem)
-    for ref, sem in ((nall, s_na), (gall, s_ga)):
-        drain(ref.at[pl.ds(0, NG - 1)], sem)
+    drain(nall.at[pl.ds(0, NG - 1)], s_na)
+    drain(gall.at[pl.ds(0, NX - 1)], s_ga)
+    for k, ref in enumerate((gbuf, ubuf, dbuf)):
+        drain(ref.at[0], s_ew.at[k])
     drain(woa.at[:, pl.ds(0, NG - 1)], s_woa)
     drain(rb.at[pl.ds(0, NP - 1)], s_rb)
     drain(fr.at[pl.ds(0, NX * NY - 1)], s_x)
     drain(fr.at[pl.ds(0, NX * NY - 1)], s_f)
-    drain(xb.at[:, 0], s_xc)
 
 
 def on_device(
@@ -561,33 +604,29 @@
     up_weight,
     down_weight,
 ):
-    y = lax.axis_index("tp")
-    half_dim = HEAD_DIM // 2
-    inverse = rotary_base ** (-jnp.arange(half_dim, dtype=F32) / half_dim)
-    gg = jnp.arange(NG)[:, None]
-    lane = jnp.arange(128)[None, :]
-    r_of = lane % 16
-    at_query = (gg % (NG // 2)) * 8 + r_of % 8
-    at_key = ((lane // 16) % 2) * 16 + gg * 2 + r_of % 2
-    entry = jnp.where(r_of < 8, at_query, at_key)
-    table = inverse[entry]
-    own = lax.dynamic_slice_in_dim(lengths, y * OWN, OWN, 0).astype(F32)
-    rows = jnp.concatenate([own, own])
-    angles = rows[None, :, None] * table[:, None, :]
-    cosine, sine = jnp.cos(angles), jnp.sin(angles)
-
     vm = pl.BlockSpec(memory_space=pltpu.VMEM)
     hbm = pl.BlockSpec(memory_space=pl.ANY)
-    smem = pl.BlockSpec(memory_space=pltpu.SMEM)
     dma = pltpu.SemaphoreType.DMA
     V = pltpu.VMEM
     scratch = [
+        V((16, 256), BF),
+        pltpu.SMEM((16,), jnp.int32),
+        V((8, 256), BF),
+        V((2, 256), BF),
+        V((2, 256), BF),
+        V((8, 256), BF),
+        V((128,), F32),
+        pltpu.SMEM((HEADS,), F32),
+        V((256,), BF),
+        V((256,), BF),
+        V((CHOSEN, 16), jnp.int32),
+        V((CHOSEN, 16), F32),
         V((OWN, CACHE, 256), BF),
         V((OWN, CACHE, 256), BF),
-        V((1, WIDTH, 128), BF),
-        V((1, WIDTH, 128), BF),
-        V((1, 128, WIDTH), BF),
-        dma((5,)),
+        V((NC, WIDTH, 128), BF),
+        V((NC, WIDTH, 128), BF),
+        V((NC, 128, WIDTH), BF),
+        dma((17,)),
         V((16, 256), BF),
         V((NZ, 16, 256), BF),
         V((8, 256), BF),
@@ -601,6 +640,8 @@
         V((NP, 8, 128), F32),
         V((NP, 8, 128), F32),
         V((1024, 512), BF),
+        V((NG, 8, 128), F32),
+        V((NG, 8, 128), F32),
         V((8, 256), F32),
         V((NY, 8, 256), F32),
         V((16, 512), F32),
@@ -612,32 +653,24 @@
         V((NZ, SLOTS, 128), F32),
         V((NZ, SLOTS, 128), F32),
         V((32, 128), F32),
-        V((NG, 32, 128), F32),
-        V((NZ, SLOTS, 256), F32),
-        V((NZ, SLOTS, 256), F32),
-        V((NX, NC, NY, 32, 256), BF),
+        V((NX, 32, 128), F32),
+        V((NZ, SLOTS, 256), BF),
+        V((NZ, SLOTS, 256), BF),
         V((NX, NY, 32, 256), BF),
         V((NX, NY, 32, 256), BF),
-        V((NX, NY, 32, 256), F32),
         V((NX * NY, 32, 256), BF),
-        V((NZ, SLOTS, 256), F32),
-        V((NZ, SLOTS, 256), F32),
+        V((NZ, SLOTS, 256), BF),
+        V((NZ, SLOTS, 256), BF),
     ]
-    sems = [dma] * 36
-    sems[27] = dma((NX * NY,))
-    out, nk, nv = pl.pallas_call(
+    sems = [dma] * 34
+    sems[28] = sems[29] = dma((3,))
+    results = pl.pallas_call(
         kernel,
-        out_shape=(
-            jax.ShapeDtypeStruct((16, 256), BF),
-            jax.ShapeDtypeStruct((16, 256), BF),
-            jax.ShapeDtypeStruct((16, 256), BF),
-        ),
-        in_specs=[vm, hbm, hbm, smem] + [vm] * 11 + [hbm] * 3 + [vm] * 2,
-        out_specs=(vm, vm, vm),
+        out_shape=pltpu.VMEM((3, 16, 256), BF),
+        in_specs=[hbm] * 17,
+        out_specs=vm,
         scratch_shapes=scratch + sems,
-        compiler_params=pltpu.CompilerParams(
-            collective_id=0, has_side_effects=True, vmem_limit_bytes=40 * 2**20
-        ),
+        compiler_params=pltpu.CompilerParams(collective_id=0, has_side_effects=True),
         cost_estimate=pl.CostEstimate(flops=10**9, bytes_accessed=5 * 10**6, transcendentals=0),
     )(
         residual,
@@ -648,20 +681,17 @@
         key_weight.T,
         value_weight.T,
         out_weight.T,
-        head_gain.reshape(1, 128),
-        mix_lambda.reshape(HEADS, 1),
-        attn_gain.reshape(1, 256),
-        moe_gain.reshape(1, 256),
-        route_ids,
+        head_gain,
+        mix_lambda,
+        attn_gain,
+        moe_gain,
         route_ids.T,
-        route_logits,
+        route_logits.T,
         gate_weight,
         up_weight,
         down_weight,
-        cosine,
-        sine,
     )
-    return out, nk, nv
+    return results[0], results[1], results[2]
 
 
 def solution(mesh):

time: 85.1 us -> 68.7 us (0.81)
  the two profiles are of different devices: /device:TPU:1 before, /device:TPU:8 now
where the time goes in v2:
time: 68.7 us; the launch traced here: 68.6 us
  Pallas kernels  67.3 us (98%)
    pallas_call x1, Pallas kernels, on_device(): pl.pallas_call(kernel, out_shape=pltpu.VMEM((3, 16, 256), BF), in_specs=[...  67.3 us

profile of v2, /device:TPU:8, one launch (start us, length us, event | category | flops | bytes accessed | tf_op | source)
XLA Modules:
  0.0 68.6 jit_solution(17072973106861617054)
XLA Ops:
  0.6 67.3 %shard_map.184 = bf16[3,16,256]{2,1,0:T(8,128)(2,1)S(1)} custom-call(bf16[16,256]{1,0:T(8,128)(2,1)} %res_hbm.1, bf16[4,1024,256]{2,1,0:T(8,128)(2,1)} %ck_hbm.1, bf16[4,1024,256]{2,1,0:T(8,128)(2,1)} %cv_hbm.1, s32[16]{0:T(128)} %lens_hbm.1, bf16[8,256]{1,0:T(8,128)(2,1)} %bitcast.12, bf16[2,256]{1,0:T(2,128)(2,1)} %bitcast.16, bf16[2,256]{1,0:T(2,128)(2,1)} %bitcast.17, ...), custom_call_target="tpu_custom_call" | custom-call | flops 1000000000 | bytes 5000000 | tf_op jit(solution)/shard_map/pallas_call | solution.py:667
  67.9 0.6 slice_bitcast_fusion

commit v3 on v2

--- a/solution.py
+++ b/solution.py
@@ -87,10 +87,10 @@
     ubuf,
     dbuf,
     loc_sem,
-    wqkv,
-    wz,
-    wos,
-    woz,
+    wkv,
+    wzq,
+    wzk,
+    woy,
     woa,
     sqs,
     sqr,
@@ -107,9 +107,8 @@
     kvo,
     hb,
     hr,
+    heads,
     lhs,
-    ob,
-    orr,
     gz_s,
     gz_r,
     gown,
@@ -121,8 +120,10 @@
     fr,
     zs,
     zr,
-    s_wz,
-    r_wz,
+    s_wzq,
+    r_wzq,
+    s_wzk,
+    r_wzk,
     s_wo,
     r_wo,
     s_woa,
@@ -139,8 +140,8 @@
     r_kv,
     s_h,
     r_h,
-    s_o,
-    r_o,
+    s_woc,
+    r_woc,
     s_gz,
     r_gz,
     s_ga,
@@ -162,11 +163,16 @@
     y = lax.axis_index("tp")
     g = x * NC + c
     p = g * NY + y
+    twin = x * NC + 1 - c
     q16 = x * NY + y
 
     def plane_id(other):
         og = lax.div(other, NY)
         return {"ep_1": lax.div(og, NC), "ep_2": lax.rem(og, NC), "tp": lax.rem(other, NY)}
+
+    def along_z(k):
+        dest = lax.rem(z + far_first(k, NZ), NZ)
+        return dest, {"ep_0": dest, "ep_2": 1 - c}
 
     def to(src, dst, ssem, rsem, dev):
         pltpu.make_async_remote_copy(
@@ -180,9 +186,18 @@
 
     @pl.loop(0, NZ - 1)
     def _(k):
-        pl.semaphore_signal(
-            barrier, inc=1, device_id={"ep_0": lax.rem(z + far_first(k, NZ), NZ)}, device_id_type=MESH
-        )
+        pl.semaphore_signal(barrier, inc=1, device_id=along_z(k)[1], device_id_type=MESH)
+
+    @pl.loop(0, 4)
+    def _(k):
+        source = 4 * y + k
+
+        @pl.when(source != z)
+        def _():
+            @pl.loop(1, NY)
+            def _(j):
+                dev = {"ep_0": source, "ep_2": 1 - c, "tp": lax.rem(y + j, NY)}
+                pl.semaphore_signal(barrier, inc=1, device_id=dev, device_id_type=MESH)
 
     @pl.loop(1, NP)
     def _(k):
@@ -222,18 +237,7 @@
         copy.start()
     for copy in small:
         copy.wait()
-    wqkv[...] = jnp.concatenate(
-        [
-            wq_ref[...].astype(F32),
-            wk_ref[...].astype(F32),
-            wv_ref[...].astype(F32),
-            jnp.zeros((4, 256), F32),
-        ],
-        axis=0,
-    ).astype(BF)
-    wz[z] = wqkv[...]
-    wos[...] = wo_ref[...]
-    woz[z] = wo_ref[...]
+    wkv[...] = jnp.concatenate([wk_ref[...].astype(F32), wv_ref[...].astype(F32)], axis=0).astype(BF)
     stream = res_ref[...].astype(F32)
     own_squares = jnp.broadcast_to(jnp.sum(stream * stream, axis=1, keepdims=True), (16, 128))
     sqs[...] = own_squares
@@ -261,43 +265,40 @@
     )
     for k in range(NZ):
         gz_s[k] = slot_gates[2 * k : 2 * k + 2]
-    gz_r[z] = gz_s[z]
 
     row = iota((1024, 256), 0)
     col = iota((1024, 256), 1)
-    src_g = lax.shift_right_logical(row, 7)
-    src_z = jnp.bitwise_and(lax.shift_right_logical(row, 4), 7)
-    src_r = jnp.bitwise_and(row, 15)
-    to_query = jnp.logical_and(src_r < 8, jnp.bitwise_and(col, 63) == src_g * 8 + src_r)
+    src_g = jnp.bitwise_xor(lax.shift_right_logical(row, 7), 1)
+    src_lane = jnp.bitwise_and(row, 127)
+    to_query = jnp.bitwise_and(col, 63) == src_g * 8 + jnp.bitwise_and(src_lane, 7)
     ebuf[:, 0:256] = jnp.where(to_query, 1.0, 0.0).astype(BF)
-    spot = src_z * 16 + src_g * 2
-    to_key = jnp.logical_and(
-        jnp.logical_and(src_r >= 8, src_r < 10), col == spot + src_r - 8
-    )
-    to_value = jnp.logical_and(
-        jnp.logical_and(src_r >= 10, src_r < 12), col == 128 + spot + src_r - 10
-    )
-    ebuf[:, 256:512] = jnp.where(jnp.logical_or(to_key, to_value), 1.0, 0.0).astype(BF)
+    src_r = jnp.bitwise_and(src_lane, 3)
+    spot = lax.shift_right_logical(src_lane, 2) * 16 + src_g * 2 + jnp.bitwise_and(src_r, 1)
+    on_spot = jnp.logical_and(col == spot, src_lane < 64)
+    ebuf[:, 256:512] = jnp.where(jnp.logical_and(on_spot, src_r < 2), 1.0, 0.0).astype(BF)
+    ebuf[:, 512:768] = jnp.where(jnp.logical_and(on_spot, src_r >= 2), 1.0, 0.0).astype(BF)
 
     lane = iota((8, 128), 1)
     sub = iota((8, 128), 0)
-    r_of = jnp.bitwise_and(lane, 15)
     place = jnp.zeros((8, 128), F32)
     for s in range(OWN):
         place = jnp.where(
             jnp.bitwise_and(sub, 3) == s, lens_ref[y * OWN + s].astype(F32), place
         )
     for k in range(NG):
-        at_query = (k % (NG // 2)) * 8 + jnp.bitwise_and(r_of, 7)
-        at_key = jnp.bitwise_and(lax.shift_right_logical(lane, 4), 1) * 16 + k * 2 + (
-            jnp.bitwise_and(r_of, 1)
+        at_query = ((k ^ 1) % (NG // 2)) * 8 + jnp.bitwise_and(lane, 7)
+        at_key = (
+            jnp.bitwise_and(lax.shift_right_logical(lane, 2), 1) * 16
+            + (k ^ 1) * 2
+            + jnp.bitwise_and(lane, 1)
         )
-        entry = jnp.where(r_of < 8, at_query, at_key).astype(F32)
+        entry = jnp.where(sub < 4, at_query, at_key).astype(F32)
         angle = place * jnp.exp(entry * (-math.log(rotary_base) / (HEAD_DIM // 2)))
         cosb[k] = jnp.cos(angle)
         sinb[k] = jnp.sin(angle)
 
-    pl.semaphore_wait(barrier, NZ - 1 + NP - 1)
+    quarter = lax.div(z, 4)
+    pl.semaphore_wait(barrier, NZ - 1 + NP - 1 + jnp.where(quarter == y, 0, NZ - 1))
 
     @pl.loop(1, NY)
     def _(k):
@@ -305,9 +306,11 @@
         to(sqs, sqr.at[y], s_sq, r_sq, dev)
         to(mgs, mga.at[y], s_mg, r_mg, dev)
 
-    @pl.loop(0, NZ - 1)
-    def _(k):
-        to(wqkv, wz.at[z], s_wz, r_wz, {"ep_0": lax.rem(z + far_first(k, NZ), NZ)})
+    @pl.loop(0, NZ)
+    def _(k):
+        dev = along_z(k)[1]
+        to(wq_ref, wzq.at[z], s_wzq, r_wzq, dev)
+        to(wkv, wzk.at[z], s_wzk, r_wzk, dev)
 
     sqr[y] = own_squares
     mga[y] = mgs[...]
@@ -325,11 +328,12 @@
             {"ep_1": lax.div(other, NC), "ep_2": lax.rem(other, NC)},
         )
 
-    @pl.loop(0, NZ - 1)
-    def _(k):
-        dest = lax.rem(z + far_first(k, NZ), NZ)
-        to(wos, woz.at[z], s_wo, r_wo, {"ep_0": dest})
-        to(gz_s.at[dest], gz_r.at[z], s_gz, r_gz, {"ep_0": dest})
+    @pl.loop(0, NZ)
+    def _(k):
+        dest, dev = along_z(k)
+        wo_dev = {"ep_0": dest, "ep_2": 1 - c, "tp": quarter}
+        to(wo_ref, woy.at[y, lax.rem(z, 4)], s_wo, r_wo, wo_dev)
+        to(gz_s.at[dest], gz_r.at[k], s_gz, r_gz, dev)
 
     partner = {"ep_2": 1 - c}
     for k, ref in enumerate((gbuf, ubuf, dbuf)):
@@ -337,11 +341,15 @@
         to(ref.at[c], ref.at[c], s_ew.at[k], r_ew.at[k], partner)
 
     drain(nall.at[pl.ds(0, NG - 1)], r_na)
-    drain(wz.at[pl.ds(0, NZ - 1)], r_wz)
-    partial = nt(nall[...].reshape(128, 256), wz[...].reshape(256, 256))
+    drain(wzq, r_wzq)
+    drain(wzk, r_wzk)
+    tokens = nall[...].reshape(128, 256)
+    part_q = nt(tokens, wzq[...].reshape(128, 256))
+    part_kv = nt(tokens, wzk[...].reshape(64, 256))
+    part_kv = jnp.concatenate([part_kv, jnp.zeros((128, 64), F32)], axis=1)
     for k in range(NP):
-        sb[k, 0:4, :] = partial[4 * k : 4 * k + 4, 0:128]
-        sb[k, 4:8, :] = partial[4 * k : 4 * k + 4, 128:256]
+        sb[k, 0:4, :] = part_q[4 * k : 4 * k + 4]
+        sb[k, 4:8, :] = part_kv[4 * k : 4 * k + 4]
 
     @pl.loop(1, NP)
     def _(k):
@@ -350,42 +358,42 @@
 
     rb[p] = sb[p]
 
-    drain(woz.at[pl.ds(0, NZ - 1)], r_wo)
-    drain(gz_r.at[pl.ds(0, NZ - 1)], r_gz)
+    drain(gz_r, r_gz)
     for k in range(NZ):
         gown[2 * k : 2 * k + 2, :] = gz_r[k]
     gall[x] = gown[...]
-    woa[:, g] = woz[...]
-
-    @pl.loop(1, NG)
-    def _(k):
-        other = lax.rem(g + k, NG)
-        dev = {"ep_1": lax.div(other, NC), "ep_2": lax.rem(other, NC)}
-        to(woz, woa.at[:, g], s_woa, r_woa, dev)
 
     @pl.loop(1, NX)
     def _(k):
         to(gown, gall.at[x], s_ga, r_ga, {"ep_1": lax.rem(x + k, NX)})
+
+    drain(woy, r_wo)
+    woa[:, :, twin] = woy[...]
+    to(woy, woa.at[:, :, twin], s_woc, r_woc, partner)
+
+    @pl.loop(1, NX)
+    def _(k):
+        to(woy, woa.at[:, :, twin], s_woa, r_woa, {"ep_1": lax.rem(x + k, NX)})
 
     drain(rb.at[pl.ds(0, NP - 1)], r_rb)
     parts = rb[...].reshape(NG, NY, 8, 128)
     raw = parts[:, 0] + parts[:, 1] + parts[:, 2] + parts[:, 3]
-    is_query = r_of < 8
-    is_key = jnp.logical_and(r_of >= 8, r_of < 10)
-    low_key = jnp.bitwise_and(lane, 63) < 32
+    is_query = sub < 4
+    is_key = jnp.logical_and(lane < 64, jnp.bitwise_and(lane, 3) < 2)
+    low_key = jnp.bitwise_and(lane, 15) < 8
     turned = []
     for k in range(NG):
         own = raw[k]
         pair = raw[(k + NG // 2) % NG]
         if k < NG // 2:
             pair = -pair
-        above = pltpu.roll(own, 96, 1)
-        below = pltpu.roll(own, 32, 1)
+        above = pltpu.roll(own, 120, 1)
+        below = pltpu.roll(own, 8, 1)
         key_pair = jnp.where(low_key, -above, below)
         spun = own * cosb[k] + jnp.where(is_query, pair, key_pair) * sinb[k]
         turned.append(jnp.where(jnp.logical_or(is_query, is_key), spun, own))
     rows8 = jnp.concatenate([t.astype(BF) for t in turned], axis=1)
-    placed = nn(rows8, ebuf[:, 256:512])
+    placed = nn(rows8, ebuf[:, 256:768])
     kvs[...] = placed
     kvr[y] = placed
 
@@ -393,21 +401,17 @@
     def _(k):
         to(kvs, kvr.at[y], s_kv, r_kv, {"tp": lax.rem(y + k, NY)})
 
-    own_keys = jnp.concatenate([placed[0:4, 0:128], placed[4:8, 0:128]], axis=1)
-    own_values = jnp.concatenate([placed[0:4, 128:256], placed[4:8, 128:256]], axis=1)
+    own_keys = placed[4:8, 0:256]
+    own_values = placed[4:8, 256:512]
 
     pieces = []
     for s in range(OWN):
         for m in range(2):
-            keep = jnp.logical_and(
-                is_query,
-                lax.shift_right_logical(lane, 4) == jnp.bitwise_and(2 * sub + m, 7),
-            )
+            keep = lax.shift_right_logical(lane, 3) == 2 * sub + m
             line = []
             for k in range(NG):
-                low = jnp.broadcast_to(turned[k][s : s + 1, :], (8, 128))
-                high = jnp.broadcast_to(turned[k][4 + s : 5 + s, :], (8, 128))
-                line.append(jnp.where(keep, jnp.where(sub < 4, low, high), 0.0))
+                whole = jnp.broadcast_to(turned[k][s : s + 1, :], (8, 128))
+                line.append(jnp.where(keep, whole, 0.0))
             pieces.append(jnp.concatenate(line, axis=1))
     spread = nn(jnp.concatenate(pieces, axis=0).astype(BF), ebuf[:, 0:256])
     for copy in caches:
@@ -446,143 +450,148 @@
         )
         rounded = contrast.astype(BF).astype(F32)
         for h in range(HEADS):
-            hb[h // 2, h % 2, s : s + 1, :] = rounded[h : h + 1, :]
-
-    hr[y] = hb[y]
+            hb[h, s : s + 1, :] = rounded[h : h + 1, :]
+
+    hr[y] = hb[...]
 
     @pl.loop(1, NY)
     def _(k):
-        other = lax.rem(y + k, NY)
-        to(hb.at[other], hr.at[y], s_h, r_h, {"tp": other})
-
-    drain(woa.at[:, pl.ds(0, NG - 1)], r_woa)
+        to(hb, hr.at[y], s_h, r_h, {"tp": lax.rem(y + k, NY)})
+
+    drain(woa.at[:, :, pl.ds(0, NX - 1)], r_woa)
+
+    @pl.loop(1, NX)
+    def _(k):
+        block = woa.at[:, :, lax.rem(x + k, NX) * NC + 1 - c]
+        to(block, block, s_woc, r_woc, partner)
+
     drain(hr.at[pl.ds(0, NY - 1)], r_h)
+    drain(woa.at[:, :, pl.ds(0, NX)], r_woc)
     for k in range(NY):
-        lhs[4 * k : 4 * k + 4, 0:128] = hr[k, 0]
-        lhs[4 * k : 4 * k + 4, 128:256] = hr[k, 1]
-    projected = nt(lhs[0:16].astype(BF), woa[...].reshape(WIDTH, 256))
+        for h in range(HEADS):
+            heads[4 * k : 4 * k + 4, 128 * h : 128 * h + 128] = hr[k, h]
+    lined = heads[...].astype(BF)
+    attended = jnp.zeros((16, 256), F32)
     for k in range(NY):
-        ob[k] = projected[:, 256 * k : 256 * k + 256]
-
-    @pl.loop(1, NY)
-    def _(k):
-        other = lax.rem(y + k, NY)
-        to(ob.at[other], orr.at[y], s_o, r_o, {"tp": other})
-
-    orr[y] = ob[y]
-    drain(orr.at[pl.ds(0, NY - 1)], r_o)
-    attended = orr[0] + orr[1] + orr[2] + orr[3]
+        attended = attended + nt(lined[:, 256 * k : 256 * k + 256], woa[k].reshape(256, 256))
     middle = (stream + attended).astype(BF)
 
     routed = nn(dispatch.astype(BF), middle)
     for k in range(NZ):
         ds[k] = routed[2 * k : 2 * k + 2].astype(ds.dtype)
-    dr[z] = ds[z]
-
-    @pl.loop(0, NZ - 1)
-    def _(k):
-        dest = lax.rem(z + far_first(k, NZ), NZ)
-        to(ds.at[dest], dr.at[z], s_d, r_d, {"ep_0": dest})
-
-    drain(dr.at[pl.ds(0, NZ - 1)], r_d)
-    for k in range(NZ):
-        lhs[2 * k : 2 * k + 2, :] = dr[k].astype(F32)
-    xb[x, y] = lhs[...].astype(BF)
-
-    @pl.loop(1, NX * NY)
-    def _(k):
-        other = lax.rem(q16 + k, NX * NY)
-        to(
-            xb.at[x, y], xb.at[x, y], s_x, r_x,
-            {"ep_1": lax.div(other, NY), "tp": lax.rem(other, NY)},
-        )
-
+
+    @pl.loop(0, NZ)
+    def _(k):
+        dest, dev = along_z(k)
+        to(ds.at[dest], dr.at[k], s_d, r_d.at[lax.div(k, 8)], dev)
+
+    rows = NX * 16
+
+    def spread(b):
+        drain(dr.at[pl.ds(8 * b, 8)], r_d.at[b])
+        for k in range(8):
+            lhs[2 * k : 2 * k + 2, :] = dr[8 * b + k].astype(F32)
+        xb[b, x, y] = lhs[0:16].astype(BF)
+
+        @pl.loop(1, NX * NY)
+        def _(k):
+            other = lax.rem(q16 + k, NX * NY)
+            to(
+                xb.at[b, x, y], xb.at[b, x, y], s_x.at[b], r_x.at[b],
+                {"ep_1": lax.div(other, NY), "tp": lax.rem(other, NY)},
+            )
+
+    def run_experts(b):
+        wide = [xb[b, :, k].reshape(rows, 256).astype(F32) for k in range(NY)]
+        total_sq = jnp.zeros((rows, 1), F32)
+        for k in range(NY):
+            total_sq = total_sq + jnp.sum(wide[k] * wide[k], axis=1, keepdims=True)
+        scale = lax.rsqrt(total_sq / WIDTH + norm_eps)
+        mixed_in = [(wide[k] * scale * mga[k, 0:1, :]).astype(BF) for k in range(NY)]
+        member = gall[:, 16 * b : 16 * b + 16, :].reshape(rows, 128)
+        produced = jnp.zeros((rows, WIDTH), F32)
+        for e in range(NC):
+            gate_act = jnp.zeros((rows, 128), F32)
+            up_act = jnp.zeros((rows, 128), F32)
+            for k in range(NY):
+                gate_act = gate_act + nn(mixed_in[k], gbuf[e, 256 * k : 256 * k + 256, :])
+                up_act = up_act + nn(mixed_in[k], ubuf[e, 256 * k : 256 * k + 256, :])
+            hidden = (gate_act / (1.0 + jnp.exp(-gate_act)) * up_act).astype(BF)
+            slot_gate = jnp.sum(
+                jnp.where(iota((rows, 128), 1) == x * NC + e, member, 0.0), axis=1, keepdims=True
+            )
+            produced = produced + nn(hidden, dbuf[e]) * slot_gate
+        for k in range(NX):
+            for j in range(NY):
+                fs[b, k, j] = produced[16 * k : 16 * k + 16, 256 * j : 256 * j + 256].astype(BF)
+
+        @pl.loop(1, NX * NY)
+        def _(k):
+            other = lax.rem(q16 + k, NX * NY)
+            ox, oy = lax.div(other, NY), lax.rem(other, NY)
+            to(fs.at[b, ox, oy], fr.at[b, q16], s_f.at[b], r_f.at[b], {"ep_1": ox, "tp": oy})
+
+        fr[b, q16] = fs[b, x, y]
+
+    def give_back(b):
+        drain(fr.at[b, pl.ds(0, NX * NY - 1)], r_f.at[b])
+        mixture = fr[b, 0].astype(F32)
+        for k in range(1, NX * NY):
+            mixture = mixture + fr[b, k].astype(F32)
+        for k in range(8):
+            zs[8 * b + k] = mixture[2 * k : 2 * k + 2].astype(zs.dtype)
+
+        @pl.loop(8 * b, 8 * b + 8)
+        def _(k):
+            source = lax.rem(z + 2 * NZ - far_first(k, NZ), NZ)
+            to(zs.at[k], zr.at[z], s_z, r_z, {"ep_0": source, "ep_2": 1 - c})
+
+    spread(1)
+    spread(0)
     drain(gall.at[pl.ds(0, NX - 1)], r_ga)
     drain(mga.at[pl.ds(0, NY - 1)], r_mg)
     for k, ref in enumerate((gbuf, ubuf, dbuf)):
         drain(ref.at[0], r_ew.at[k])
-    drain(fr.at[pl.ds(0, NX * NY - 1)], r_x)
-
-    rows = NX * 32
-    wide = [xb[:, k].reshape(rows, 256).astype(F32) for k in range(NY)]
-    total_sq = jnp.zeros((rows, 1), F32)
-    for k in range(NY):
-        total_sq = total_sq + jnp.sum(wide[k] * wide[k], axis=1, keepdims=True)
-    scale = lax.rsqrt(total_sq / WIDTH + norm_eps)
-    mixed_in = [(wide[k] * scale * mga[k, 0:1, :]).astype(BF) for k in range(NY)]
-    produced = jnp.zeros((rows, WIDTH), F32)
-    for e in range(NC):
-        gate_act = jnp.zeros((rows, 128), F32)
-        up_act = jnp.zeros((rows, 128), F32)
-        for k in range(NY):
-            gate_act = gate_act + nn(mixed_in[k], gbuf[e, 256 * k : 256 * k + 256, :])
-            up_act = up_act + nn(mixed_in[k], ubuf[e, 256 * k : 256 * k + 256, :])
-        hidden = (gate_act / (1.0 + jnp.exp(-gate_act)) * up_act).astype(BF)
-        slot_gate = jnp.sum(
-            jnp.where(iota((rows, 128), 1) == x * NC + e, gall[...].reshape(rows, 128), 0.0),
-            axis=1,
-            keepdims=True,
-        )
-        produced = produced + nn(hidden, dbuf[e]) * slot_gate
-
-    for k in range(NX):
-        for j in range(NY):
-            fs[k, j] = produced[32 * k : 32 * k + 32, 256 * j : 256 * j + 256].astype(BF)
-
-    @pl.loop(1, NX * NY)
-    def _(k):
-        other = lax.rem(q16 + k, NX * NY)
-        ox, oy = lax.div(other, NY), lax.rem(other, NY)
-        to(fs.at[ox, oy], fr.at[q16], s_f, r_f, {"ep_1": ox, "tp": oy})
-
-    fr[q16] = fs[x, y]
-    drain(fr.at[pl.ds(0, NX * NY - 1)], r_f)
-    mixture = fr[0].astype(F32)
-    for k in range(1, NX * NY):
-        mixture = mixture + fr[k].astype(F32)
-    for k in range(NZ):
-        zs[k] = mixture[2 * k : 2 * k + 2].astype(zs.dtype)
-    zr[z] = zs[z]
-
-    @pl.loop(0, NZ - 1)
-    def _(k):
-        dest = lax.rem(z + far_first(k, NZ), NZ)
-        to(zs.at[dest], zr.at[z], s_z, r_z, {"ep_0": dest})
+    drain(fr.at[1, pl.ds(0, NX * NY - 1)], r_x.at[1])
+    run_experts(1)
+    drain(fr.at[0, pl.ds(0, NX * NY - 1)], r_x.at[0])
+    run_experts(0)
+    give_back(1)
+    give_back(0)
 
     drain(kvr.at[pl.ds(0, NY - 1)], r_kv)
     for k in range(NY):
-        for half in range(2):
-            kvo[4 * k : 4 * k + 4, 128 * half : 128 * half + 128] = kvr[k, 4 * half : 4 * half + 4, 0:128]
-            kvo[4 * k : 4 * k + 4, 256 + 128 * half : 384 + 128 * half] = kvr[
-                k, 4 * half : 4 * half + 4, 128:256
-            ]
+        kvo[4 * k : 4 * k + 4, :] = kvr[k, 4:8, :]
     out_ref[1] = kvo[:, 0:256].astype(BF)
     out_ref[2] = kvo[:, 256:512].astype(BF)
 
-    drain(zr.at[pl.ds(0, NZ - 1)], r_z)
+    drain(zr, r_z)
     for k in range(NZ):
         lhs[2 * k : 2 * k + 2, :] = zr[k].astype(F32)
     mix = nn(combine.astype(BF), lhs[...].astype(BF))
     out_ref[0] = (middle.astype(F32) + mix).astype(BF)
 
     for ref, sem in (
-        (wz, s_wz),
-        (woz, s_wo),
+        (wzq, s_wzq),
+        (wzk, s_wzk),
+        (woy, s_wo),
         (gz_r, s_gz),
         (dr, s_d),
         (zr, s_z),
     ):
-        drain(ref.at[pl.ds(0, NZ - 1)], sem)
-    for ref, sem in ((sqr, s_sq), (mga, s_mg), (kvr, s_kv), (hr, s_h), (orr, s_o)):
+        drain(ref, sem)
+    for ref, sem in ((sqr, s_sq), (mga, s_mg), (kvr, s_kv), (hr, s_h)):
         drain(ref.at[pl.ds(0, NY - 1)], sem)
     drain(nall.at[pl.ds(0, NG - 1)], s_na)
     drain(gall.at[pl.ds(0, NX - 1)], s_ga)
     for k, ref in enumerate((gbuf, ubuf, dbuf)):
         drain(ref.at[0], s_ew.at[k])
-    drain(woa.at[:, pl.ds(0, NG - 1)], s_woa)
+    drain(woa.at[:, :, pl.ds(0, NX - 1)], s_woa)
+    drain(woa.at[:, :, pl.ds(0, NX)], s_woc)
     drain(rb.at[pl.ds(0, NP - 1)], s_rb)
-    drain(fr.at[pl.ds(0, NX * NY - 1)], s_x)
-    drain(fr.at[pl.ds(0, NX * NY - 1)], s_f)
+    for b in range(2):
+        drain(fr.at[b, pl.ds(0, NX * NY - 1)], s_x.at[b])
+        drain(fr.at[b, pl.ds(0, NX * NY - 1)], s_f.at[b])
 
 
 def on_device(
@@ -627,11 +636,11 @@
         V((NC, WIDTH, 128), BF),
         V((NC, 128, WIDTH), BF),
         dma((17,)),
-        V((16, 256), BF),
-        V((NZ, 16, 256), BF),
-        V((8, 256), BF),
+        V((4, 256), BF),
         V((NZ, 8, 256), BF),
-        V((NZ, NG, 8, 256), BF),
+        V((NZ, 4, 256), BF),
+        V((NY, NZ // NY, 8, 256), BF),
+        V((NY, NZ // NY, NG, 8, 256), BF),
         V((16, 128), F32),
         V((NY, 16, 128), F32),
         V((NG, 16, 256), BF),
@@ -639,31 +648,31 @@
         V((NY, 8, 256), F32),
         V((NP, 8, 128), F32),
         V((NP, 8, 128), F32),
-        V((1024, 512), BF),
+        V((1024, 768), BF),
         V((NG, 8, 128), F32),
         V((NG, 8, 128), F32),
-        V((8, 256), F32),
-        V((NY, 8, 256), F32),
+        V((8, 512), F32),
+        V((NY, 8, 512), F32),
         V((16, 512), F32),
-        V((NY, 2, OWN, 128), F32),
-        V((NY, 2, OWN, 128), F32),
+        V((HEADS, OWN, 128), F32),
+        V((NY, HEADS, OWN, 128), F32),
+        V((16, WIDTH), F32),
         V((32, 256), F32),
-        V((NY, 16, 256), F32),
-        V((NY, 16, 256), F32),
         V((NZ, SLOTS, 128), F32),
         V((NZ, SLOTS, 128), F32),
         V((32, 128), F32),
         V((NX, 32, 128), F32),
         V((NZ, SLOTS, 256), BF),
         V((NZ, SLOTS, 256), BF),
-        V((NX, NY, 32, 256), BF),
-        V((NX, NY, 32, 256), BF),
-        V((NX * NY, 32, 256), BF),
+        V((2, NX, NY, 16, 256), BF),
+        V((2, NX, NY, 16, 256), BF),
+        V((2, NX * NY, 16, 256), BF),
         V((NZ, SLOTS, 256), BF),
         V((NZ, SLOTS, 256), BF),
     ]
-    sems = [dma] * 34
-    sems[28] = sems[29] = dma((3,))
+    sems = [dma] * 36
+    sems[30] = sems[31] = dma((3,))
+    sems[27] = sems[28] = sems[29] = sems[32] = sems[33] = dma((2,))
     results = pl.pallas_call(
         kernel,
         out_shape=pltpu.VMEM((3, 16, 256), BF),

time: 68.7 us -> 64.4 us (0.937)
  the two profiles are of different devices: /device:TPU:8 before, /device:TPU:1 now
where the time goes in v3:
time: 64.4 us; the launch traced here: 64.2 us
  Pallas kernels  63 us (98%)
  between operations  0.65 us (1%)
    pallas_call x1, Pallas kernels, on_device(): pl.pallas_call(kernel, out_shape=pltpu.VMEM((3, 16, 256), BF), in_specs=[...  63 us

profile of v3, /device:TPU:1, one launch (start us, length us, event | category | flops | bytes accessed | tf_op | source)
XLA Modules:
  0.0 64.2 jit_solution(3081510140313712428)
XLA Ops:
  0.6 63.0 %shard_map.184 = bf16[3,16,256]{2,1,0:T(8,128)(2,1)S(1)} custom-call(bf16[16,256]{1,0:T(8,128)(2,1)} %res_hbm.1, bf16[4,1024,256]{2,1,0:T(8,128)(2,1)} %ck_hbm.1, bf16[4,1024,256]{2,1,0:T(8,128)(2,1)} %cv_hbm.1, s32[16]{0:T(128)} %lens_hbm.1, bf16[8,256]{1,0:T(8,128)(2,1)} %bitcast.12, bf16[2,256]{1,0:T(2,128)(2,1)} %bitcast.16, bf16[2,256]{1,0:T(2,128)(2,1)} %bitcast.17, ...), custom_call_target="tpu_custom_call" | custom-call | flops 1000000000 | bytes 5000000 | tf_op jit(solution)/shard_map/pallas_call | solution.py:676
  63.6 0.6 slice_bitcast_fusion

commit v4 on v3

--- a/solution.py
+++ b/solution.py
@@ -90,6 +90,7 @@
     wkv,
     wzq,
     wzk,
+    woz,
     woy,
     woa,
     sqs,
@@ -107,7 +108,6 @@
     kvo,
     hb,
     hr,
-    heads,
     lhs,
     gz_s,
     gz_r,
@@ -126,6 +126,8 @@
     r_wzk,
     s_wo,
     r_wo,
+    s_wo2,
+    r_wo2,
     s_woa,
     r_woa,
     s_sq,
@@ -142,6 +144,8 @@
     r_h,
     s_woc,
     r_woc,
+    s_woy,
+    r_woy,
     s_gz,
     r_gz,
     s_ga,
@@ -174,6 +178,11 @@
         dest = lax.rem(z + far_first(k, NZ), NZ)
         return dest, {"ep_0": dest, "ep_2": 1 - c}
 
+    def in_plane(k):
+        ox = lax.rem(x + far_first(lax.div(k, NY), NX), NX)
+        oy = lax.rem(y + far_first(lax.rem(k, NY), NY), NY)
+        return ox, oy
+
     def to(src, dst, ssem, rsem, dev):
         pltpu.make_async_remote_copy(
             src_ref=src, dst_ref=dst, send_sem=ssem, recv_sem=rsem, device_id=dev, device_id_type=MESH
@@ -184,22 +193,16 @@
 
     barrier = pltpu.get_barrier_semaphore()
 
-    @pl.loop(0, NZ - 1)
+    @pl.loop(0, NZ - 1, unroll=True)
     def _(k):
         pl.semaphore_signal(barrier, inc=1, device_id=along_z(k)[1], device_id_type=MESH)
 
-    @pl.loop(0, 4)
-    def _(k):
-        source = 4 * y + k
-
-        @pl.when(source != z)
-        def _():
-            @pl.loop(1, NY)
-            def _(j):
-                dev = {"ep_0": source, "ep_2": 1 - c, "tp": lax.rem(y + j, NY)}
-                pl.semaphore_signal(barrier, inc=1, device_id=dev, device_id_type=MESH)
-
-    @pl.loop(1, NP)
+    for step in (1, 14, 15):
+        pl.semaphore_signal(
+            barrier, inc=1, device_id={"ep_0": lax.rem(z + step, NZ)}, device_id_type=MESH
+        )
+
+    @pl.loop(1, NP, unroll=True)
     def _(k):
         pl.semaphore_signal(
             barrier, inc=1, device_id=plane_id(lax.rem(p + k, NP)), device_id_type=MESH
@@ -297,16 +300,20 @@
         cosb[k] = jnp.cos(angle)
         sinb[k] = jnp.sin(angle)
 
-    quarter = lax.div(z, 4)
-    pl.semaphore_wait(barrier, NZ - 1 + NP - 1 + jnp.where(quarter == y, 0, NZ - 1))
-
-    @pl.loop(1, NY)
+    pl.semaphore_wait(barrier, NZ - 1 + NP - 1 + 3)
+
+    @pl.loop(1, NY, unroll=True)
     def _(k):
         dev = {"tp": lax.rem(y + k, NY)}
         to(sqs, sqr.at[y], s_sq, r_sq, dev)
         to(mgs, mga.at[y], s_mg, r_mg, dev)
 
-    @pl.loop(0, NZ)
+    z_low, z_high = lax.rem(z, 4), lax.div(z, 4)
+    for step in (8, 4, 12, 0):
+        dev = {"ep_0": lax.rem(z + step, NZ), "ep_2": 1 - c}
+        to(wo_ref, woz.at[z_low, z_high], s_wo, r_wo, dev)
+
+    @pl.loop(0, NZ, unroll=True)
     def _(k):
         dev = along_z(k)[1]
         to(wq_ref, wzq.at[z], s_wzq, r_wzq, dev)
@@ -320,7 +327,7 @@
     normed = (stream * scale * again_ref[...].astype(F32).reshape(1, 256)).astype(BF)
     nall[g] = normed
 
-    @pl.loop(1, NG)
+    @pl.loop(1, NG, unroll=True)
     def _(k):
         other = lax.rem(g + k, NG)
         to(
@@ -328,19 +335,22 @@
             {"ep_1": lax.div(other, NC), "ep_2": lax.rem(other, NC)},
         )
 
-    @pl.loop(0, NZ)
+    @pl.loop(0, NZ, unroll=True)
     def _(k):
         dest, dev = along_z(k)
-        wo_dev = {"ep_0": dest, "ep_2": 1 - c, "tp": quarter}
-        to(wo_ref, woy.at[y, lax.rem(z, 4)], s_wo, r_wo, wo_dev)
         to(gz_s.at[dest], gz_r.at[k], s_gz, r_gz, dev)
 
     partner = {"ep_2": 1 - c}
+    for copy in experts:
+        copy.wait()
     for k, ref in enumerate((gbuf, ubuf, dbuf)):
-        experts[k].wait()
         to(ref.at[c], ref.at[c], s_ew.at[k], r_ew.at[k], partner)
 
     drain(nall.at[pl.ds(0, NG - 1)], r_na)
+    drain(woz.at[0], r_wo)
+    for step in (2, 1, 15):
+        to(woz.at[z_low], woz.at[z_low], s_wo2, r_wo2, {"ep_0": lax.rem(z + step, NZ)})
+
     drain(wzq, r_wzq)
     drain(wzk, r_wzk)
     tokens = nall[...].reshape(128, 256)
@@ -351,29 +361,35 @@
         sb[k, 0:4, :] = part_q[4 * k : 4 * k + 4]
         sb[k, 4:8, :] = part_kv[4 * k : 4 * k + 4]
 
-    @pl.loop(1, NP)
-    def _(k):
-        other = lax.rem(p + k, NP)
+    @pl.loop(0, NX * NY, unroll=True)
+    def _(k):
+        ox, oy = in_plane(k)
+        other = (ox * NC + 1 - c) * NY + oy
         to(sb.at[other], rb.at[p], s_rb, r_rb, plane_id(other))
 
+        @pl.when(k < NX * NY - 1)
+        def _():
+            same = (ox * NC + c) * NY + oy
+            to(sb.at[same], rb.at[p], s_rb, r_rb, plane_id(same))
+
     rb[p] = sb[p]
+
+    drain(woz.at[pl.ds(0, 3)], r_wo2)
+    woy[y] = woz[:, y]
+
+    @pl.loop(1, NY, unroll=True)
+    def _(k):
+        other = lax.rem(y + k, NY)
+        to(woz.at[:, other], woy.at[y], s_woy, r_woy, {"tp": other})
 
     drain(gz_r, r_gz)
     for k in range(NZ):
         gown[2 * k : 2 * k + 2, :] = gz_r[k]
     gall[x] = gown[...]
 
-    @pl.loop(1, NX)
+    @pl.loop(1, NX, unroll=True)
     def _(k):
         to(gown, gall.at[x], s_ga, r_ga, {"ep_1": lax.rem(x + k, NX)})
-
-    drain(woy, r_wo)
-    woa[:, :, twin] = woy[...]
-    to(woy, woa.at[:, :, twin], s_woc, r_woc, partner)
-
-    @pl.loop(1, NX)
-    def _(k):
-        to(woy, woa.at[:, :, twin], s_woa, r_woa, {"ep_1": lax.rem(x + k, NX)})
 
     drain(rb.at[pl.ds(0, NP - 1)], r_rb)
     parts = rb[...].reshape(NG, NY, 8, 128)
@@ -397,7 +413,7 @@
     kvs[...] = placed
     kvr[y] = placed
 
-    @pl.loop(1, NY)
+    @pl.loop(1, NY, unroll=True)
     def _(k):
         to(kvs, kvr.at[y], s_kv, r_kv, {"tp": lax.rem(y + k, NY)})
 
@@ -414,6 +430,14 @@
                 line.append(jnp.where(keep, whole, 0.0))
             pieces.append(jnp.concatenate(line, axis=1))
     spread = nn(jnp.concatenate(pieces, axis=0).astype(BF), ebuf[:, 0:256])
+    drain(woy.at[pl.ds(0, NY - 1)], r_woy)
+    woa[:, :, twin] = woy[...]
+    to(woy, woa.at[:, :, twin], s_woc, r_woc, partner)
+
+    for k in (2, 1, 3):
+        dev = {"ep_1": lax.rem(x + k, NX), "ep_2": 1 - c}
+        to(woy, woa.at[:, :, twin], s_woa, r_woa.at[k - 1], dev)
+
     for copy in caches:
         copy.wait()
     blk = lax.shift_right_logical(iota((16, 256), 1), 6)
@@ -450,27 +474,22 @@
         )
         rounded = contrast.astype(BF).astype(F32)
         for h in range(HEADS):
-            hb[h, s : s + 1, :] = rounded[h : h + 1, :]
+            hb[s : s + 1, 128 * h : 128 * h + 128] = rounded[h : h + 1, :]
 
     hr[y] = hb[...]
 
-    @pl.loop(1, NY)
+    @pl.loop(1, NY, unroll=True)
     def _(k):
         to(hb, hr.at[y], s_h, r_h, {"tp": lax.rem(y + k, NY)})
 
-    drain(woa.at[:, :, pl.ds(0, NX - 1)], r_woa)
-
-    @pl.loop(1, NX)
-    def _(k):
-        block = woa.at[:, :, lax.rem(x + k, NX) * NC + 1 - c]
+    for k in (1, 3, 2):
+        block = woa.at[:, :, lax.rem(x + NX - k, NX) * NC + c]
+        drain(block, r_woa.at[k - 1])
         to(block, block, s_woc, r_woc, partner)
 
     drain(hr.at[pl.ds(0, NY - 1)], r_h)
     drain(woa.at[:, :, pl.ds(0, NX)], r_woc)
-    for k in range(NY):
-        for h in range(HEADS):
-            heads[4 * k : 4 * k + 4, 128 * h : 128 * h + 128] = hr[k, h]
-    lined = heads[...].astype(BF)
+    lined = hr[...].reshape(16, WIDTH).astype(BF)
     attended = jnp.zeros((16, 256), F32)
     for k in range(NY):
         attended = attended + nt(lined[:, 256 * k : 256 * k + 256], woa[k].reshape(256, 256))
@@ -480,7 +499,7 @@
     for k in range(NZ):
         ds[k] = routed[2 * k : 2 * k + 2].astype(ds.dtype)
 
-    @pl.loop(0, NZ)
+    @pl.loop(0, NZ, unroll=True)
     def _(k):
         dest, dev = along_z(k)
         to(ds.at[dest], dr.at[k], s_d, r_d.at[lax.div(k, 8)], dev)
@@ -493,13 +512,10 @@
             lhs[2 * k : 2 * k + 2, :] = dr[8 * b + k].astype(F32)
         xb[b, x, y] = lhs[0:16].astype(BF)
 
-        @pl.loop(1, NX * NY)
+        @pl.loop(0, NX * NY - 1, unroll=True)
         def _(k):
-            other = lax.rem(q16 + k, NX * NY)
-            to(
-                xb.at[b, x, y], xb.at[b, x, y], s_x.at[b], r_x.at[b],
-                {"ep_1": lax.div(other, NY), "tp": lax.rem(other, NY)},
-            )
+            ox, oy = in_plane(k)
+            to(xb.at[b, x, y], xb.at[b, x, y], s_x.at[b], r_x.at[b], {"ep_1": ox, "tp": oy})
 
     def run_experts(b):
         wide = [xb[b, :, k].reshape(rows, 256).astype(F32) for k in range(NY)]
@@ -525,10 +541,9 @@
             for j in range(NY):
                 fs[b, k, j] = produced[16 * k : 16 * k + 16, 256 * j : 256 * j + 256].astype(BF)
 
-        @pl.loop(1, NX * NY)
+        @pl.loop(0, NX * NY - 1, unroll=True)
         def _(k):
-            other = lax.rem(q16 + k, NX * NY)
-            ox, oy = lax.div(other, NY), lax.rem(other, NY)
+            ox, oy = in_plane(k)
             to(fs.at[b, ox, oy], fr.at[b, q16], s_f.at[b], r_f.at[b], {"ep_1": ox, "tp": oy})
 
         fr[b, q16] = fs[b, x, y]
@@ -541,7 +556,7 @@
         for k in range(8):
             zs[8 * b + k] = mixture[2 * k : 2 * k + 2].astype(zs.dtype)
 
-        @pl.loop(8 * b, 8 * b + 8)
+        @pl.loop(8 * b, 8 * b + 8, unroll=True)
         def _(k):
             source = lax.rem(z + 2 * NZ - far_first(k, NZ), NZ)
             to(zs.at[k], zr.at[z], s_z, r_z, {"ep_0": source, "ep_2": 1 - c})
@@ -574,13 +589,14 @@
     for ref, sem in (
         (wzq, s_wzq),
         (wzk, s_wzk),
-        (woy, s_wo),
+        (woz.at[0], s_wo),
+        (woz.at[pl.ds(0, 3)], s_wo2),
         (gz_r, s_gz),
         (dr, s_d),
         (zr, s_z),
     ):
         drain(ref, sem)
-    for ref, sem in ((sqr, s_sq), (mga, s_mg), (kvr, s_kv), (hr, s_h)):
+    for ref, sem in ((sqr, s_sq), (mga, s_mg), (kvr, s_kv), (hr, s_h), (woy, s_woy)):
         drain(ref.at[pl.ds(0, NY - 1)], sem)
     drain(nall.at[pl.ds(0, NG - 1)], s_na)
     drain(gall.at[pl.ds(0, NX - 1)], s_ga)
@@ -639,6 +655,7 @@
         V((4, 256), BF),
         V((NZ, 8, 256), BF),
         V((NZ, 4, 256), BF),
+        V((4, NZ // 4, 8, 256), BF),
         V((NY, NZ // NY, 8, 256), BF),
         V((NY, NZ // NY, NG, 8, 256), BF),
         V((16, 128), F32),
@@ -654,9 +671,8 @@
         V((8, 512), F32),
         V((NY, 8, 512), F32),
         V((16, 512), F32),
-        V((HEADS, OWN, 128), F32),
-        V((NY, HEADS, OWN, 128), F32),
-        V((16, WIDTH), F32),
+        V((OWN, WIDTH), F32),
+        V((NY, OWN, WIDTH), F32),
         V((32, 256), F32),
         V((NZ, SLOTS, 128), F32),
         V((NZ, SLOTS, 128), F32),
@@ -670,9 +686,11 @@
         V((NZ, SLOTS, 256), BF),
         V((NZ, SLOTS, 256), BF),
     ]
-    sems = [dma] * 36
-    sems[30] = sems[31] = dma((3,))
-    sems[27] = sems[28] = sems[29] = sems[32] = sems[33] = dma((2,))
+    sems = [dma] * 40
+    for k in (31, 32, 33, 36, 37):
+        sems[k] = dma((2,))
+    sems[34] = sems[35] = dma((3,))
+    sems[9] = dma((3,))
     results = pl.pallas_call(
         kernel,
         out_shape=pltpu.VMEM((3, 16, 256), BF),

time: 64.4 us -> 63.2 us (0.981)
  Pallas kernels: 63 us -> 61.8 us
    pallas_call x1, Pallas kernels: 63 us -> 61.8 us  [on_device(): pl.pallas_call(kernel, out_shape=pltpu.VMEM((3, 16, 256), BF), in_specs=[...]
where the time goes in v4:
time: 63.2 us; the launch traced here: 63 us
  Pallas kernels  61.8 us (98%)
  between operations  0.65 us (1%)
    pallas_call x1, Pallas kernels, on_device(): pl.pallas_call(kernel, out_shape=pltpu.VMEM((3, 16, 256), BF), in_specs=[...  61.8 us

profile of v4, /device:TPU:1, one launch (start us, length us, event | category | flops | bytes accessed | tf_op | source)
XLA Modules:
  0.0 63.0 jit_solution(12862082310329683169)
XLA Ops:
  0.6 61.8 %shard_map.184 = bf16[3,16,256]{2,1,0:T(8,128)(2,1)S(1)} custom-call(bf16[16,256]{1,0:T(8,128)(2,1)} %res_hbm.1, bf16[4,1024,256]{2,1,0:T(8,128)(2,1)} %ck_hbm.1, bf16[4,1024,256]{2,1,0:T(8,128)(2,1)} %cv_hbm.1, s32[16]{0:T(128)} %lens_hbm.1, bf16[8,256]{1,0:T(8,128)(2,1)} %bitcast.12, bf16[2,256]{1,0:T(2,128)(2,1)} %bitcast.16, bf16[2,256]{1,0:T(2,128)(2,1)} %bitcast.17, ...), custom_call_target="tpu_custom_call" | custom-call | flops 1000000000 | bytes 5000000 | tf_op jit(solution)/shard_map/pallas_call | solution.py:694
  62.4 0.6 slice_bitcast_fusion

commit v5 on v4

--- a/solution.py
+++ b/solution.py
@@ -376,20 +376,24 @@
 
     drain(woz.at[pl.ds(0, 3)], r_wo2)
     woy[y] = woz[:, y]
+    over_x = [(k, {"ep_1": lax.rem(x + k, NX), "ep_2": 1 - c}) for k in (2, 1, 3)]
 
     @pl.loop(1, NY, unroll=True)
     def _(k):
         other = lax.rem(y + k, NY)
         to(woz.at[:, other], woy.at[y], s_woy, r_woy, {"tp": other})
 
-    drain(gz_r, r_gz)
-    for k in range(NZ):
-        gown[2 * k : 2 * k + 2, :] = gz_r[k]
-    gall[x] = gown[...]
-
-    @pl.loop(1, NX, unroll=True)
-    def _(k):
-        to(gown, gall.at[x], s_ga, r_ga, {"ep_1": lax.rem(x + k, NX)})
+    for k, dev in over_x:
+        to(woz.at[:, y], woa.at[y, :, twin], s_woa, r_woa.at[k - 1], dev)
+
+    drain(woy.at[pl.ds(0, NY - 1)], r_woy)
+    woa[:, :, twin] = woy[...]
+    to(woy, woa.at[:, :, twin], s_woc, r_woc, partner)
+
+    for k, dev in over_x:
+        for j in range(1, NY):
+            piece = lax.rem(y + j, NY)
+            to(woy.at[piece], woa.at[piece, :, twin], s_woa, r_woa.at[k - 1], dev)
 
     drain(rb.at[pl.ds(0, NP - 1)], r_rb)
     parts = rb[...].reshape(NG, NY, 8, 128)
@@ -413,10 +417,6 @@
     kvs[...] = placed
     kvr[y] = placed
 
-    @pl.loop(1, NY, unroll=True)
-    def _(k):
-        to(kvs, kvr.at[y], s_kv, r_kv, {"tp": lax.rem(y + k, NY)})
-
     own_keys = placed[4:8, 0:256]
     own_values = placed[4:8, 256:512]
 
@@ -430,14 +430,6 @@
                 line.append(jnp.where(keep, whole, 0.0))
             pieces.append(jnp.concatenate(line, axis=1))
     spread = nn(jnp.concatenate(pieces, axis=0).astype(BF), ebuf[:, 0:256])
-    drain(woy.at[pl.ds(0, NY - 1)], r_woy)
-    woa[:, :, twin] = woy[...]
-    to(woy, woa.at[:, :, twin], s_woc, r_woc, partner)
-
-    for k in (2, 1, 3):
-        dev = {"ep_1": lax.rem(x + k, NX), "ep_2": 1 - c}
-        to(woy, woa.at[:, :, twin], s_woa, r_woa.at[k - 1], dev)
-
     for copy in caches:
         copy.wait()
     blk = lax.shift_right_logical(iota((16, 256), 1), 6)
@@ -449,32 +441,43 @@
     lam = jnp.zeros((8, 128), F32)
     for h in range(HEADS):
         lam = jnp.where(sub == h, lam_ref[h], lam)
+    queries = [jnp.where(blk == own_block, spread[16 * s : 16 * s + 16], 0.0) for s in range(OWN)]
+    scores = jnp.concatenate([nt(queries[s].astype(BF), kbuf[s]) for s in range(OWN)], axis=0) * 0.125
+    fresh = jnp.concatenate(
+        [jnp.sum(queries[s] * own_keys[s : s + 1], axis=1, keepdims=True) for s in range(OWN)], axis=0
+    ) * 0.125
+    seq_of = lax.shift_right_logical(iota((16 * OWN, 1), 0), 4)
+    length = jnp.zeros((16 * OWN, 1), jnp.int32)
     for s in range(OWN):
-        queries = jnp.where(blk == own_block, spread[16 * s : 16 * s + 16], 0.0)
-        scores = nt(queries.astype(BF), kbuf[s]) * 0.125
-        length = lens_ref[y * OWN + s]
-        scores = jnp.where(iota((16, CACHE), 1) < length, scores, masked_score)
-        fresh = jnp.sum(queries * own_keys[s : s + 1], axis=1, keepdims=True) * 0.125
-        top = jnp.maximum(jnp.max(scores, axis=1, keepdims=True), fresh)
-        weights = jnp.exp(scores - top).astype(BF)
-        fresh_weight = jnp.exp(fresh - top).astype(BF).astype(F32)
-        total = jnp.sum(weights.astype(F32), axis=1, keepdims=True) + fresh_weight
-        mixed = nn(weights, vbuf[s])
+        length = jnp.where(seq_of == s, lens_ref[y * OWN + s], length)
+    scores = jnp.where(iota((16 * OWN, CACHE), 1) < length, scores, masked_score)
+    top = jnp.maximum(jnp.max(scores, axis=1, keepdims=True), fresh)
+    weights = jnp.exp(scores - top).astype(BF)
+    fresh_weight = jnp.exp(fresh - top).astype(BF).astype(F32)
+    total = jnp.sum(weights.astype(F32), axis=1, keepdims=True) + fresh_weight
+    mixed = [nn(weights[16 * s : 16 * s + 16], vbuf[s]) for s in range(OWN)]
+    contrasts = []
+    for s in range(OWN):
+        here = slice(16 * s, 16 * s + 16)
+        fresh_here = fresh_weight[here]
         values = jnp.where(
             head_low,
-            mixed[:, 0:128] + fresh_weight * own_values[s : s + 1, 0:128],
-            mixed[:, 128:256] + fresh_weight * own_values[s : s + 1, 128:256],
+            mixed[s][:, 0:128] + fresh_here * own_values[s : s + 1, 0:128],
+            mixed[s][:, 128:256] + fresh_here * own_values[s : s + 1, 128:256],
         )
-        averaged = values / total
-        contrast = averaged[0:8] - lam * averaged[8:16]
-        contrast = (
-            contrast
-            * lax.rsqrt(jnp.mean(contrast * contrast, axis=1, keepdims=True) + head_eps)
-            * hgain_ref[...].reshape(1, 128)
-        )
-        rounded = contrast.astype(BF).astype(F32)
+        averaged = values / total[here]
+        contrasts.append(averaged[0:8] - lam * averaged[8:16])
+    contrast = jnp.concatenate(contrasts, axis=0)
+    contrast = (
+        contrast
+        * lax.rsqrt(jnp.mean(contrast * contrast, axis=1, keepdims=True) + head_eps)
+        * hgain_ref[...].reshape(1, 128)
+    )
+    rounded = contrast.astype(BF).astype(F32)
+    for s in range(OWN):
         for h in range(HEADS):
-            hb[s : s + 1, 128 * h : 128 * h + 128] = rounded[h : h + 1, :]
+            at = HEADS * s + h
+            hb[s : s + 1, 128 * h : 128 * h + 128] = rounded[at : at + 1, :]
 
     hr[y] = hb[...]
 
@@ -503,6 +506,19 @@
     def _(k):
         dest, dev = along_z(k)
         to(ds.at[dest], dr.at[k], s_d, r_d.at[lax.div(k, 8)], dev)
+
+    drain(gz_r, r_gz)
+    for k in range(NZ):
+        gown[2 * k : 2 * k + 2, :] = gz_r[k]
+    gall[x] = gown[...]
+
+    @pl.loop(1, NX, unroll=True)
+    def _(k):
+        to(gown, gall.at[x], s_ga, r_ga, {"ep_1": lax.rem(x + k, NX)})
+
+    @pl.loop(1, NY, unroll=True)
+    def _(k):
+        to(kvs, kvr.at[y], s_kv, r_kv, {"tp": lax.rem(y + k, NY)})
 
     rows = NX * 16
 

time: 63.2 us -> 62.5 us (0.989)
  Pallas kernels: 61.8 us -> 61.1 us
    pallas_call x1, Pallas kernels: 61.8 us -> 61.1 us  [on_device(): pl.pallas_call(kernel, out_shape=pltpu.VMEM((3, 16, 256), BF), in_specs=[...]
where the time goes in v5:
time: 62.5 us; the launch traced here: 62.4 us
  Pallas kernels  61.1 us (98%)
  between operations  0.65 us (1%)
    pallas_call x1, Pallas kernels, on_device(): pl.pallas_call(kernel, out_shape=pltpu.VMEM((3, 16, 256), BF), in_specs=[...  61.1 us

profile of v5, /device:TPU:1, one launch (start us, length us, event | category | flops | bytes accessed | tf_op | source)
XLA Modules:
  0.0 62.4 jit_solution(2283741471838940089)
XLA Ops:
  0.6 61.1 %shard_map.184 = bf16[3,16,256]{2,1,0:T(8,128)(2,1)S(1)} custom-call(bf16[16,256]{1,0:T(8,128)(2,1)} %res_hbm.1, bf16[4,1024,256]{2,1,0:T(8,128)(2,1)} %ck_hbm.1, bf16[4,1024,256]{2,1,0:T(8,128)(2,1)} %cv_hbm.1, s32[16]{0:T(128)} %lens_hbm.1, bf16[8,256]{1,0:T(8,128)(2,1)} %bitcast.12, bf16[2,256]{1,0:T(2,128)(2,1)} %bitcast.16, bf16[2,256]{1,0:T(2,128)(2,1)} %bitcast.17, ...), custom_call_target="tpu_custom_call" | custom-call | flops 1000000000 | bytes 5000000 | tf_op jit(solution)/shard_map/pallas_call | solution.py:710
  61.8 0.6 slice_bitcast_fusion

commit v6 on v5

--- a/solution.py
+++ b/solution.py
@@ -387,13 +387,13 @@
         to(woz.at[:, y], woa.at[y, :, twin], s_woa, r_woa.at[k - 1], dev)
 
     drain(woy.at[pl.ds(0, NY - 1)], r_woy)
-    woa[:, :, twin] = woy[...]
-    to(woy, woa.at[:, :, twin], s_woc, r_woc, partner)
-
     for k, dev in over_x:
         for j in range(1, NY):
             piece = lax.rem(y + j, NY)
             to(woy.at[piece], woa.at[piece, :, twin], s_woa, r_woa.at[k - 1], dev)
+
+    to(woy, woa.at[:, :, twin], s_woc, r_woc, partner)
+    woa[:, :, twin] = woy[...]
 
     drain(rb.at[pl.ds(0, NP - 1)], r_rb)
     parts = rb[...].reshape(NG, NY, 8, 128)

time: 62.5 us -> 62.5 us (level)
  no operation moved by 1% of the time
where the time goes in v6:
time: 62.5 us; the launch traced here: 62.4 us
  Pallas kernels  61.1 us (98%)
  between operations  0.65 us (1%)
    pallas_call x1, Pallas kernels, on_device(): pl.pallas_call(kernel, out_shape=pltpu.VMEM((3, 16, 256), BF), in_specs=[...  61.1 us

profile of v6, /device:TPU:1, one launch (start us, length us, event | category | flops | bytes accessed | tf_op | source)
XLA Modules:
  0.0 62.4 jit_solution(11975009996990558430)
XLA Ops:
  0.6 61.1 %shard_map.184 = bf16[3,16,256]{2,1,0:T(8,128)(2,1)S(1)} custom-call(bf16[16,256]{1,0:T(8,128)(2,1)} %res_hbm.1, bf16[4,1024,256]{2,1,0:T(8,128)(2,1)} %ck_hbm.1, bf16[4,1024,256]{2,1,0:T(8,128)(2,1)} %cv_hbm.1, s32[16]{0:T(128)} %lens_hbm.1, bf16[8,256]{1,0:T(8,128)(2,1)} %bitcast.12, bf16[2,256]{1,0:T(2,128)(2,1)} %bitcast.16, bf16[2,256]{1,0:T(2,128)(2,1)} %bitcast.17, ...), custom_call_target="tpu_custom_call" | custom-call | flops 1000000000 | bytes 5000000 | tf_op jit(solution)/shard_map/pallas_call | solution.py:710
  61.8 0.6 slice_bitcast_fusion
